TPU v7x, 32 devices: a whole 2x2x4 slice. The times are simulated.
32 devices in a mesh: sp: 16 (over z, y, x), tp: 2 (over core).
Axes of the slice: x: 2, y: 2, z: 4, core: 2. Of those that a mesh axis runs over, the one named last changes fastest.
Arguments:
- mid_stream: bfloat16 [5120, 2048], P('sp', 'tp'), may hold values from -6 to 6
- layer_cot: bfloat16 [5120, 2048], P('sp', 'tp'), may hold values from -6 to 6
- ffn_gain: bfloat16 [2048], P('tp'), may hold values from 0.099609375 to 1.8984375
- expert_ids: int32 [5120, 2], P('sp'), may hold values from 0 to 15, all different within a row; in each aligned block of 320 rows (0 to 319, 320 to 639, ...) at most 80 rows name the same one
- group_prob: float32 [5120], P('sp'), may hold values from 0.25 to 1
- first_share: float32 [5120], P('sp'), may hold values from 0.5 to 0.95
- expert_gate: bfloat16 [16, 2048, 1024], P('sp', None, 'tp'), may hold values from -0.125 to 0.125
- expert_up: bfloat16 [16, 2048, 1024], P('sp', None, 'tp'), may hold values from -0.125 to 0.125
- expert_down: bfloat16 [16, 1024, 2048], P('sp', 'tp'), may hold values from -0.1875 to 0.1875
- out_weight: bfloat16 [2048, 1024], P(None, 'tp'), may hold values from -0.1875 to 0.1875
- conv_gain: bfloat16 [1024], P('tp'), may hold values from 0.099609375 to 1.8984375
- b_gate: bfloat16 [5120, 1024], P('sp', 'tp'), may hold values from -6 to 6
- c_gate: bfloat16 [5120, 1024], P('sp', 'tp'), may hold values from -6 to 6
- conv_in: bfloat16 [5120, 1024], P('sp', 'tp'), may hold values from -6 to 6
- conv_out: bfloat16 [5120, 1024], P('sp', 'tp'), may hold values from -6 to 6
- conv_taps: bfloat16 [3, 1024], P(None, 'tp'), may hold values from -3.5 to 3.5
Outputs:
- grad_gate: float32 [16, 2048, 1024], P('sp', None, 'tp')
- grad_up: float32 [16, 2048, 1024], P('sp', None, 'tp')
- grad_down: float32 [16, 1024, 2048], P('sp', 'tp')
- grad_out_weight: float32 [2048, 1024], P('sp', 'tp')
- mid_grad: bfloat16 [5120, 2048], P('sp', 'tp')
- grad_b: bfloat16 [5120, 1024], P('sp', 'tp')
- grad_c: bfloat16 [5120, 1024], P('sp', 'tp')
- grad_conv_in: bfloat16 [5120, 1024], P('sp', 'tp')
Inputs may be any that keep to these rules, and one draw needn't show every extreme that they name: `expert_ids`: each row names 2 different experts. Among the rows of one device no expert is named more than 80 times, a bound that some block reaches.
All inputs are finite; a program needn't handle non-finite values.
Results may differ from a plain program's by a relative error of at most 0.0067.
Values may be sent and summed in bfloat16 or wider, within the bound.
No kernel may reach another device: no remote copies, remote signals or barrier semaphores. Data moves between devices by JAX's collectives and lax.ppermute only.
A program may use at most 128 MiB of HBM per device.

v0:
```python
import jax
import jax.numpy as jnp
from jax import lax
from jax.sharding import PartitionSpec as P

D = 2048
GROUP = 64


epsilon = 1e-06


def from_behind(block, axis, distance):
    devices = range(lax.axis_size(axis))
    route = [(i - distance, i) for i in devices if i - distance in devices]
    return lax.ppermute(block, axis, route)


def silu_parts(pre):
    sigma = jax.nn.sigmoid(pre)
    return (pre * sigma, sigma * (1.0 + pre * (1.0 - sigma)))


def contract_rows(left, right):
    return lax.dot_general(
        left, right, (((0,), (0,)), ((), ())), preferred_element_type=jnp.float32
    )


def contract_cols(left, right):
    return lax.dot_general(
        left, right, (((1,), (1,)), ((), ())), preferred_element_type=jnp.float32
    )


def expert_pass(token_rows, cot_rows, expert_gate, expert_up, expert_down):
    moved_tokens, moved_cots = (
        lax.all_to_all(token_rows, "sp", split_axis=0, concat_axis=0, tiled=True),
        lax.all_to_all(cot_rows, "sp", split_axis=0, concat_axis=0, tiled=True),
    )
    full_tokens, full_cots = (
        lax.all_gather(moved_tokens, "tp", axis=2, tiled=True),
        lax.all_gather(moved_cots, "tp", axis=2, tiled=True),
    )
    local_count = expert_gate.shape[0]
    source_count = full_tokens.shape[0] // local_count
    slot_count = full_tokens.shape[1]
    split_tokens = full_tokens.reshape(source_count, local_count, slot_count, D)
    split_cots = full_cots.reshape(source_count, local_count, slot_count, D)
    tokens_in = split_tokens[:, 0].reshape(source_count * slot_count, D)
    cots_in = split_cots[:, 0].reshape(source_count * slot_count, D)
    gate_w = expert_gate[0]
    up_w = expert_up[0]
    pre_gate = jnp.dot(tokens_in, gate_w, preferred_element_type=jnp.float32)
    pre_up = jnp.dot(tokens_in, up_w, preferred_element_type=jnp.float32)
    active, slope = silu_parts(pre_gate)
    hidden = (active * pre_up).astype(jnp.bfloat16)
    down_grads = [contract_rows(hidden, cots_in)]
    d_hidden = contract_cols(cots_in, expert_down[0])
    d_gate = (d_hidden * pre_up * slope).astype(jnp.bfloat16)
    d_up = (d_hidden * active).astype(jnp.bfloat16)
    gate_grads = [contract_rows(tokens_in, d_gate)]
    up_grads = [contract_rows(tokens_in, d_up)]
    partial_term = contract_cols(d_gate, gate_w) + contract_cols(d_up, up_w)
    partials = [partial_term.reshape(source_count, slot_count, D)]
    stacked = jnp.stack(partials, axis=1).reshape(source_count * local_count, slot_count, D)
    summed = lax.psum_scatter(stacked.astype(jnp.bfloat16), "tp", scatter_dimension=2, tiled=True)
    returned = lax.all_to_all(summed, "sp", split_axis=0, concat_axis=0, tiled=True)
    grads = (
        jnp.stack(gate_grads, axis=0),
        jnp.stack(up_grads, axis=0),
        jnp.stack(down_grads, axis=0),
    )
    return (returned, grads)


def shards(
    mid_stream,
    layer_cot,
    ffn_gain,
    expert_ids,
    group_prob,
    first_share,
    expert_gate,
    expert_up,
    expert_down,
    out_weight,
    conv_gain,
    b_gate,
    c_gate,
    conv_in,
    conv_out,
    conv_taps,
):
    row_count = mid_stream.shape[0]
    half_width = mid_stream.shape[1]
    expert_count = lax.axis_size("sp") * expert_gate.shape[0]
    slot_count = 4 * row_count // expert_count
    mid32 = mid_stream.astype(jnp.float32)
    gain32 = ffn_gain.astype(jnp.float32)
    square_sum = lax.psum(jnp.sum(mid32 * mid32, axis=1), "tp")
    inv_rms = lax.rsqrt(square_sum / D + epsilon)
    normed = (mid32 * inv_rms[:, None] * gain32).astype(jnp.bfloat16)
    shares = jnp.stack([group_prob * first_share, group_prob * (1.0 - first_share)], axis=1)
    weighted = (layer_cot.astype(jnp.float32)[:, None, :] * shares[:, :, None]).astype(jnp.bfloat16)
    flat_ids = expert_ids.reshape(-1)
    pair_count = flat_ids.shape[0]
    onehot = (flat_ids[:, None] == jnp.arange(expert_count, dtype=jnp.int32)[None, :]).astype(
        jnp.int32
    )
    before = jnp.cumsum(onehot, axis=0) - onehot
    ranks = jnp.sum(before * onehot, axis=1)
    slot_index = flat_ids * slot_count + ranks
    source = jnp.full((expert_count * slot_count,), pair_count, jnp.int32)
    source = source.at[slot_index].set(jnp.arange(pair_count, dtype=jnp.int32))
    normed_pad = jnp.concatenate([normed, jnp.zeros((1, half_width), jnp.bfloat16)], axis=0)
    weighted_pad = jnp.concatenate(
        [weighted.reshape(pair_count, half_width), jnp.zeros((1, half_width), jnp.bfloat16)], axis=0
    )
    token_rows = normed_pad[source // 2].reshape(expert_count, slot_count, half_width)
    cot_rows = weighted_pad[source].reshape(expert_count, slot_count, half_width)
    back_rows, grads = expert_pass(token_rows, cot_rows, expert_gate, expert_up, expert_down)
    picked = back_rows.reshape(expert_count * slot_count, half_width)[slot_index]
    d_normed = jnp.sum(picked.astype(jnp.float32).reshape(row_count, 2, half_width), axis=1)
    g_dn = gain32 * d_normed
    inner = lax.psum(jnp.sum(mid32 * g_dn, axis=1), "tp") / D
    mid_total = (
        layer_cot.astype(jnp.float32)
        + inv_rms[:, None] * g_dn
        - mid32 * (inv_rms**3 * inner)[:, None]
    )
    mid_grad = mid_total.astype(jnp.bfloat16)
    full_mid = lax.all_gather(mid_grad, "tp", axis=1, tiled=True)
    channel_count = b_gate.shape[1]
    b32 = b_gate.astype(jnp.float32)
    y32 = conv_out.astype(jnp.float32)
    grouped = (b32 * y32).reshape(row_count, channel_count // GROUP, GROUP)
    group_rms = lax.rsqrt(jnp.mean(grouped * grouped, axis=-1) + epsilon)
    cgain = conv_gain.astype(jnp.float32).reshape(channel_count // GROUP, GROUP)
    conv_normed = (
        (grouped * group_rms[..., None] * cgain)
        .reshape(row_count, channel_count)
        .astype(jnp.bfloat16)
    )
    grad_out_weight = lax.psum_scatter(
        contract_rows(full_mid, conv_normed), "sp", scatter_dimension=0, tiled=True
    )
    d_normed_conv = jnp.dot(full_mid, out_weight, preferred_element_type=jnp.float32).reshape(
        grouped.shape
    )
    g_dc = cgain * d_normed_conv
    group_inner = jnp.mean(grouped * g_dc, axis=-1)
    d_gated = (
        group_rms[..., None] * g_dc - grouped * (group_rms**3 * group_inner)[..., None]
    ).reshape(row_count, channel_count)
    grad_b = (d_gated * y32).astype(jnp.bfloat16)
    d_conv_out = d_gated * b32
    following = from_behind(d_conv_out[:2], "sp", -1)
    extended = jnp.concatenate([d_conv_out, following], axis=0)
    taps = conv_taps.astype(jnp.float32)
    d_mixed = taps[2] * extended[:-2] + taps[1] * extended[1:-1] + taps[0] * extended[2:]
    grad_c = (d_mixed * conv_in.astype(jnp.float32)).astype(jnp.bfloat16)
    grad_conv_in = (d_mixed * c_gate.astype(jnp.float32)).astype(jnp.bfloat16)
    return (grads[0], grads[1], grads[2], grad_out_weight, mid_grad, grad_b, grad_c, grad_conv_in)


def solution(mesh):
    placed = (
        P("sp", "tp"),
        P("sp", "tp"),
        P("tp"),
        P("sp", None),
        P("sp"),
        P("sp"),
        P("sp", None, "tp"),
        P("sp", None, "tp"),
        P("sp", "tp", None),
        P(None, "tp"),
        P("tp"),
        P("sp", "tp"),
        P("sp", "tp"),
        P("sp", "tp"),
        P("sp", "tp"),
        P(None, "tp"),
    )
    return jax.shard_map(
        shards,
        mesh=mesh,
        in_specs=placed,
        out_specs=(
            P("sp", None, "tp"),
            P("sp", None, "tp"),
            P("sp", "tp", None),
            P("sp", "tp"),
            P("sp", "tp"),
            P("sp", "tp"),
            P("sp", "tp"),
            P("sp", "tp"),
        ),
        check_vma=False,
    )
```

profile of v0, /device:TPU:0, one launch (start us, length us, event | category | flops | bytes accessed | tf_op | source)
XLA Modules:
  0.0 422.6 jit_solution(15122894277143947482)
XLA Ops:
  7.2 0.8 broadcast_multiply_fusion
  8.0 0.8 copy.25
  9.1 0.7 convert_element_type.80
  9.8 1.3 fusion.10
  11.1 2.6 psum.14
  14.1 1.4 reduce-window.6
  15.9 4.1 scatter_custom_fusion
  20.0 1.3 fusion.12
  21.4 5.1 %gather_fusion = bf16[1280,1024]{1,0:T(8,128)(2,1)} fusion(bf16[321,1024]{1,0:T(8,128)(2,1)S(1)} %concatenate.9, s32[2048]{0:T(1024)S(1)} %get-tuple-element.26), kind=kCustom, calls=%fused_computation | custom fusion | bytes 5248000 | tf_op jit(solution)/shard_map/gather | solution.py:120
  26.5 8.4 %all-to-all-start = ((bf16[16,80,1024]{2,1,0:T(8,128)(2,1)}), bf16[16,80,1024]{2,1,0:T(8,128)(2,1)}, u32[]{:S(2)}, u32[]{:S(2)}) async-start(bf16[16,80,1024]{2,1,0:T(8,128)(2,1)} %bitcast.71), calls=%async_computation | async-start | bytes 5242880 | tf_op jit(solution)/shard_map/all_to_all | solution.py:38
  35.0 52.0 %all-to-all-done = bf16[16,80,1024]{2,1,0:T(8,128)(2,1)} async-done(((bf16[16,80,1024]{2,1,0:T(8,128)(2,1)}), bf16[16,80,1024]{2,1,0:T(8,128)(2,1)}, u32[]{:S(2)}, u32[]{:S(2)}) %all-to-all-start) | async-done | bytes 2621472 | tf_op jit(solution)/shard_map/all_to_all | solution.py:38
  87.1 2.2 mul.227
  89.2 4.5 %mul.228 = f32[640,1024]{1,0:T(8,128)} reshape(f32[320,2,1024]{2,1,0:T(2,128)} %mul.227) | data formatting | bytes 5242880 | tf_op jit(solution)/shard_map/mul | solution.py:105
  94.1 1.9 multiply_convert_fusion.3
  96.1 5.1 %gather_fusion.1 = bf16[1280,1024]{1,0:T(8,128)(2,1)} fusion(bf16[641,1024]{1,0:T(8,128)(2,1)S(1)} %concatenate.10, s32[2048]{0:T(1024)S(1)} %get-tuple-element.25), kind=kCustom, calls=%fused_computation.1 | custom fusion | bytes 5248000 | tf_op jit(solution)/shard_map/gather | solution.py:121
  101.2 72.9 %all_to_all.15 = bf16[16,80,1024]{2,1,0:T(8,128)(2,1)} all-to-all(bf16[16,80,1024]{2,1,0:T(8,128)(2,1)} %bitcast.72), channel_id=1, replica_groups=mesh['sp'=16,'tp'=2] {'sp'}, dimensions={0} | all-to-all | bytes 5242880 | tf_op jit(solution)/shard_map/all_to_all | solution.py:39
  174.4 7.0 %fusion.3 = f32[1280,512]{1,0:T(8,128)} fusion(bf16[1280,2048]{1,0:T(8,128)(2,1)} %bitcast.80, bf16[1,2048,512]{2,1,0:T(8,128)(2,1)S(1)} %copy-done), kind=kOutput, calls=%fused_computation.20 | convolution fusion | flops 2684354560 | bytes 9961472 | tf_op jit(solution)/shard_map/dot_general | solution.py:54
  181.4 4.4 %fusion.6 = f32[1280,512]{1,0:T(8,128)} fusion(bf16[1280,2048]{1,0:T(8,128)(2,1)S(1)} %bitcast.83, bf16[1,2048,512]{2,1,0:T(8,128)(2,1)S(1)} %copy-done.15), kind=kOutput, calls=%fused_computation.23 | convolution fusion | flops 2684354560 | bytes 9961472 | tf_op jit(solution)/shard_map/dot_general | solution.py:55
  185.8 2.0 all-gather.6.cloned.1.call-done
  187.9 8.4 %multiply_convert_fusion.1 = (bf16[1280,512]{1,0:T(8,128)(2,1)S(1)}, bf16[1280,512]{1,0:T(8,128)(2,1)S(1)}) fusion(f32[1280,512]{1,0:T(8,128)} %fusion.3, f32[1280,512]{1,0:T(8,128)} %fusion.6, bf16[1280,2048]{1,0:T(8,128)(2,1)} %bitcast.84, bf16[1,512,2048]{2,1,0:T(8,128)(2,1)} %param.24), kind=kOutput, calls=%fused_computation.9 | convolution fusion | flops 2692874240 | bytes 15204352 | tf_op jit(solution)/shard_map/dot_general | solution.py:31
  196.3 2.9 fusion.1
  199.3 4.8 %add_convert_fusion = bf16[1280,2048]{1,0:T(8,128)(2,1)} fusion(f32[1280,2048]{1,0:T(8,128)S(1)} %fusion.1, bf16[1280,512]{1,0:T(8,128)(2,1)S(1)} %get-tuple-element.14, bf16[1,2048,512]{2,1,0:T(8,128)(2,1)S(1)} %copy-done.16), kind=kOutput, calls=%fused_computation.4 | convolution fusion | flops 2689597440 | bytes 19136512 | tf_op jit(solution)/shard_map/dot_general | solution.py:31
  204.1 14.2 %reduce-scatter.3.cloned.1.call-done = bf16[16,80,1024]{2,1,0:T(8,128)(2,1)} async-done(((bf16[16,80,2048]{2,1,0:T(8,128)(2,1)}), bf16[16,80,1024]{2,1,0:T(8,128)(2,1)}) %reduce-scatter.3.cloned.1.call-update) | async-done | bytes 2621456 | tf_op jit(solution)/shard_map/reduce_scatter | solution.py:67
  218.3 6.9 %all-to-all-start.2 = ((bf16[16,80,1024]{2,1,0:T(8,128)(2,1)}), bf16[16,80,1024]{2,1,0:T(8,128)(2,1)S(1)}, u32[]{:S(2)}, u32[]{:S(2)}) async-start(bf16[16,80,1024]{2,1,0:T(8,128)(2,1)} %reduce-scatter.3.cloned.1.call-done), calls=%async_computation.3 | async-start | bytes 5242880 | tf_op jit(solution)/shard_map/all_to_all | solution.py:68
  225.5 51.8 %all-to-all-done.2 = bf16[16,80,1024]{2,1,0:T(8,128)(2,1)S(1)} async-done(((bf16[16,80,1024]{2,1,0:T(8,128)(2,1)}), bf16[16,80,1024]{2,1,0:T(8,128)(2,1)S(1)}, u32[]{:S(2)}, u32[]{:S(2)}) %all-to-all-start.2) | async-done | bytes 2621472 | tf_op jit(solution)/shard_map/all_to_all | solution.py:68
  277.3 3.5 gather_fusion.2
  280.7 4.1 reshape.120
  284.8 4.9 %reduce_sum.59 = f32[320,1024]{1,0:T(8,128)S(1)} reduce(f32[320,2,1024]{2,1,0:T(2,128)} %reshape.120, f32[]{:T(128)} %constant.15.clone.1), dimensions={1}, to_apply=%region_7.8 | reduce | flops 327680 | bytes 3932164 | tf_op jit(solution)/shard_map/reduce_sum | solution.py:124
  289.8 0.3 fusion.13
  290.1 2.5 psum.15
  292.5 1.2 fusion.15
  294.0 0.3 copy.29
  294.3 16.4 %all-gather.8.cloned.1.call-done = bf16[320,2048]{1,0:T(8,128)(2,1)} async-done(((bf16[320,1024]{1,0:T(8,128)(2,1)}), bf16[320,2048]{1,0:T(8,128)(2,1)}) %all-gather.8.cloned.1.call-update) | async-done | bytes 1310736 | tf_op jit(solution)/shard_map/all_gather | solution.py:133
  310.7 2.8 fusion.40
  313.5 0.3 copy.32
  314.6 4.7 %fusion.23 = f32[2048,512]{1,0:T(8,128)} fusion(bf16[320,2048]{1,0:T(8,128)(2,1)} %all-gather.8.cloned.1.call-done, f32[320,512]{1,0:T(8,128)S(1)} %copy.30, f32[512]{0:T(512)S(1)} %convert_element_type.96, bf16[320,512]{1,0:T(8,128)(2,1)S(1)} %copy-done.3, bf16[320,512]{1,0:T(8,128)(2,1)S(1)} %copy-done.4), kind=kOutput, calls=%fused_computation.51 | convolution fusion | flops 672071680 | bytes 6817792 | tf_op jit(solution)/shard_map/dot_general | solution.py:25
  319.3 0.7 copy-done.10
  320.0 8.0 %convolution_bitcast_fusion.2 = f32[1,2048,512]{2,1,0:T(8,128)} fusion(bf16[1280,2048]{1,0:T(8,128)(2,1)} %bitcast.81, bf16[1280,512]{1,0:T(8,128)(2,1)} %copy-done.19), kind=kOutput, calls=%fused_computation.7 | convolution fusion | flops 2684354560 | bytes 10747904 | tf_op jit(solution)/shard_map/dot_general | solution.py:25
  328.0 7.2 %convolution_bitcast_fusion.1 = f32[1,2048,512]{2,1,0:T(8,128)} fusion(bf16[1280,2048]{1,0:T(8,128)(2,1)} %bitcast.82, bf16[1280,512]{1,0:T(8,128)(2,1)S(1)} %copy-done.18), kind=kOutput, calls=%fused_computation.6 | convolution fusion | flops 2684354560 | bytes 10747904 | tf_op jit(solution)/shard_map/dot_general | solution.py:25
  335.2 4.5 %convolution_bitcast_fusion = f32[1,512,2048]{2,1,0:T(8,128)} fusion(bf16[1280,2048]{1,0:T(8,128)(2,1)S(1)} %bitcast.87, f32[1280,512]{1,0:T(8,128)S(1)} %copy-done.21, f32[1280,512]{1,0:T(8,128)S(1)} %copy-done.20), kind=kOutput, calls=%fused_computation.5 | convolution fusion | flops 2688286720 | bytes 14680064 | tf_op jit(solution)/shard_map/dot_general | solution.py:25
  339.8 1.1 copy.33
  340.9 1.7 convert_multiply_fusion.6
  342.6 1.4 collective-permute-start
  344.1 0.8 fusion.20
  344.9 3.6 collective-permute-done
  348.5 1.0 multiply_convert_fusion.5
  349.5 0.8 multiply_convert_fusion.6
  350.3 65.7 %reduce-scatter.5.cloned.1.call-done = f32[128,512]{1,0:T(8,128)} async-done(((f32[2048,512]{1,0:T(8,128)}), f32[128,512]{1,0:T(8,128)}) %reduce-scatter.5.cloned.1.call-update) | async-done | bytes 262160 | tf_op jit(solution)/shard_map/reduce_scatter | solution.py:145
  (92 shorter events, 3.3 us)
Async XLA Ops:
  7.2 167.2 %copy-start = (bf16[1,2048,512]{2,1,0:T(8,128)(2,1)S(1)}, bf16[1,2048,512]{2,1,0:T(8,128)(2,1)}, u32[]{:S(2)}) copy-start(bf16[1,2048,512]{2,1,0:T(8,128)(2,1)} %param.22) | copy-start | bytes 6291460
  26.5 8.4 %copy-start.12 = (f32[320]{0:T(512)S(1)}, f32[320]{0:T(512)}, u32[]{:S(2)}) copy-start(f32[320]{0:T(512)} %param.20) | copy-start | bytes 3844
  26.5 8.4 %copy-start.13 = (f32[320]{0:T(512)S(1)}, f32[320]{0:T(512)}, u32[]{:S(2)}) copy-start(f32[320]{0:T(512)} %param.21) | copy-start | bytes 3844
  26.5 60.5 %all-to-all-start = ((bf16[16,80,1024]{2,1,0:T(8,128)(2,1)}), bf16[16,80,1024]{2,1,0:T(8,128)(2,1)}, u32[]{:S(2)}, u32[]{:S(2)}) async-start(bf16[16,80,1024]{2,1,0:T(8,128)(2,1)} %bitcast.71), calls=%async_computation | async-start | bytes 5242880 | tf_op jit(solution)/shard_map/all_to_all | solution.py:38
  34.9 52.2 %copy-start.6 = (bf16[320,1024]{1,0:T(8,128)(2,1)S(1)}, bf16[320,1024]{1,0:T(8,128)(2,1)}, u32[]{:S(2)}) copy-start(bf16[320,1024]{1,0:T(8,128)(2,1)} %param.17) | copy-start | bytes 1966084
  34.9 139.5 %all-gather.4.cloned.1.call-start = ((), (), s32[]{:S(2)}) async-start(), calls=%async_computation.5 | async-start | bytes 7864320 | tf_op jit(solution)/shard_map/all_gather | solution.py:42
  87.0 100.9 %all-gather.6.cloned.1.call-start = ((), (), s32[]{:S(2)}) async-start(), calls=%async_computation.6 | async-start | bytes 7864320 | tf_op jit(solution)/shard_map/all_gather | solution.py:43
  174.1 44.2 %reduce-scatter.3.cloned.1.call-start = ((), (), s32[]{:S(2)}) async-start(), calls=%async_computation.7 | async-start | bytes 7864320 | tf_op jit(solution)/shard_map/reduce_scatter | solution.py:67
  174.4 7.0 %copy-start.14 = (bf16[16,80,2048]{2,1,0:T(8,128)(2,1)S(1)}, bf16[16,80,2048]{2,1,0:T(8,128)(2,1)}, u32[]{:S(2)}) copy-start(bf16[16,80,2048]{2,1,0:T(8,128)(2,1)} %all-gather.4.cloned.1.call-done) | copy-start | bytes 15728644
  174.4 7.0 %copy-start.15 = (bf16[1,2048,512]{2,1,0:T(8,128)(2,1)S(1)}, bf16[1,2048,512]{2,1,0:T(8,128)(2,1)}, u32[]{:S(2)}) copy-start(bf16[1,2048,512]{2,1,0:T(8,128)(2,1)} %param.23) | copy-start | bytes 6291460
  196.3 3.0 copy-start.19
  196.3 3.0 copy-start.17
  196.3 3.0 copy-start.16
  218.3 59.0 %all-to-all-start.2 = ((bf16[16,80,1024]{2,1,0:T(8,128)(2,1)}), bf16[16,80,1024]{2,1,0:T(8,128)(2,1)S(1)}, u32[]{:S(2)}, u32[]{:S(2)}) async-start(bf16[16,80,1024]{2,1,0:T(8,128)(2,1)} %reduce-scatter.3.cloned.1.call-done), calls=%async_computation.3 | async-start | bytes 5242880 | tf_op jit(solution)/shard_map/all_to_all | solution.py:68
  225.2 85.4 %all-gather.8.cloned.1.call-start = ((), (), s32[]{:S(2)}) async-start(), calls=%async_computation.8 | async-start | bytes 1966080 | tf_op jit(solution)/shard_map/all_gather | solution.py:133
  284.8 5.0 %copy-start.2 = (bf16[320,1024]{1,0:T(8,128)(2,1)S(1)}, bf16[320,1024]{1,0:T(8,128)(2,1)}, u32[]{:S(2)}) copy-start(bf16[320,1024]{1,0:T(8,128)(2,1)} %param.16) | copy-start | bytes 1966084
  284.8 7.7 %copy-start.7 = (bf16[320,1024]{1,0:T(8,128)(2,1)S(1)}, bf16[320,1024]{1,0:T(8,128)(2,1)}, u32[]{:S(2)}) copy-start(bf16[320,1024]{1,0:T(8,128)(2,1)} %param.17) | copy-start | bytes 1966084
  289.8 4.1 copy-start.11
  289.8 4.2 copy-start.3
  289.8 4.1 copy-start.4
  293.8 122.2 %reduce-scatter.5.cloned.1.call-start = ((), (), s32[]{:S(2)}) async-start(), calls=%async_computation.9 | async-start | bytes 4456448 | tf_op jit(solution)/shard_map/reduce_scatter | solution.py:145
  313.5 0.8 copy-start.5
  319.3 0.7 copy-start.10
  320.0 8.0 %copy-start.18 = (bf16[1280,512]{1,0:T(8,128)(2,1)S(1)}, bf16[1280,512]{1,0:T(8,128)(2,1)}, u32[]{:S(2)}) copy-start(bf16[1280,512]{1,0:T(8,128)(2,1)} %copy-done.17) | copy-start | bytes 3932164
  320.0 15.2 %slice-start = ((s8[5242880]{0:T(1024)(128)(4,1)}), s8[4194304]{0:T(1024)(128)(4,1)S(1)}, s32[]{:S(2)}) async-start(s8[5242880]{0:T(1024)(128)(4,1)} %bitcast.85), calls=%async_computation.10 | async-start | bytes 8388608
  328.0 7.2 %slice-start.1 = ((s8[5242880]{0:T(1024)(128)(4,1)}), s8[1048576]{0:T(1024)(128)(4,1)S(1)}, s32[]{:S(2)}) async-start(s8[5242880]{0:T(1024)(128)(4,1)} %bitcast.85), calls=%async_computation.11 | async-start | bytes 2097152
  328.0 7.2 %copy-start.20 = (f32[1280,512]{1,0:T(8,128)S(1)}, f32[1280,512]{1,0:T(8,128)}, u32[]{:S(2)}) copy-start(f32[1280,512]{1,0:T(8,128)} %fusion.3) | copy-start | bytes 7864324
  328.0 7.2 %copy-start.21 = (f32[1280,512]{1,0:T(8,128)S(1)}, f32[1280,512]{1,0:T(8,128)}, u32[]{:S(2)}) copy-start(f32[1280,512]{1,0:T(8,128)} %fusion.6) | copy-start | bytes 7864324
  340.9 7.6 %copy-start.9 = (bf16[320,512]{1,0:T(8,128)(2,1)S(1)}, bf16[320,512]{1,0:T(8,128)(2,1)}, u32[]{:S(2)}) copy-start(bf16[320,512]{1,0:T(8,128)(2,1)} %param.28) | copy-start | bytes 983044
  340.9 75.1 %copy-start.1 = (bf16[1,2048,512]{2,1,0:T(8,128)(2,1)S(1)}, bf16[1,2048,512]{2,1,0:T(8,128)(2,1)}, u32[]{:S(2)}) copy-start(bf16[1,2048,512]{2,1,0:T(8,128)(2,1)} %param.22) | copy-start | bytes 6291460
  342.6 6.8 %copy-start.8 = (bf16[320,512]{1,0:T(8,128)(2,1)S(1)}, bf16[320,512]{1,0:T(8,128)(2,1)}, u32[]{:S(2)}) copy-start(bf16[320,512]{1,0:T(8,128)(2,1)} %param.29) | copy-start | bytes 983044
  342.6 5.8 %collective-permute-start = (f32[2,512]{1,0:T(2,128)S(1)}, f32[2,512]{1,0:T(2,128)S(1)}, u32[]{:S(2)}, u32[]{:S(2)}) collective-permute-start(f32[2,512]{1,0:T(2,128)S(1)} %slice.41), channel_id=1, source_target_pairs={{2,0},{4,2},{6,4},{8,6},{10,8},{12,10},{14,12},{16,14},{18,16},{20... | collective-permute-start | bytes 12296 | tf_op jit(solution)/shard_map/ppermute | solution.py:16
Sparse Core Ops, SparseCore 0:
  87.1 22.5 all-gather.3
  174.2 13.5 all-gather.5
  204.2 14.0 reduce-scatter.2
  293.9 16.7 all-gather.7
  319.5 96.5 reduce-scatter.4
where the time goes:
time: 423 us
  waiting for transfers between devices  206 us (49%)
  blocking collectives  78 us (18%)
  matrix products  54.8 us (13%)
  local copies, waits for them, and re-layouts  33.6 us (8%)
  other arithmetic  18.8 us (4%)
  starting transfers between devices  17.3 us (4%)
  between operations  14.3 us (3%)
    all_to_all x1, blocking collectives, expert_pass(): lax.all_to_all(cot_rows, 'sp', split_axis=0, concat_axis=0, tiled=True)  72.9 us
    reduce_scatter x1, waiting for transfers between devices, shards(): lax.psum_scatter(contract_rows(full_mid, conv_normed), 'sp', scatter_dime...  65.7 us
    all_to_all x1, waiting for transfers between devices, expert_pass(): lax.all_to_all(token_rows, 'sp', split_axis=0, concat_axis=0, tiled=True)  52 us
    all_to_all x1, waiting for transfers between devices, expert_pass(): lax.all_to_all(summed, 'sp', split_axis=0, concat_axis=0, tiled=True)  51.8 us
    dot_general x4, matrix products, contract_rows(): lax.dot_general(left, right, (((0,), (0,)), ((), ())), preferred_element_...  24.4 us
    all_gather x1, waiting for transfers between devices, shards(): full_mid = lax.all_gather(mid_grad, 'tp', axis=1, tiled=True)  16.4 us
    dot_general x3, matrix products, contract_cols(): lax.dot_general(left, right, (((1,), (1,)), ((), ())), preferred_element_...  16.2 us
    reduce_scatter x1, waiting for transfers between devices, expert_pass(): lax.psum_scatter(stacked.astype(jnp.bfloat16), 'tp', scatter_dimension=2,...  14.2 us
  transfers between devices with their start and end apart: 8, of which 7 were waited for; matrix products, arithmetic and copies ran while one was open for 12% of the time, Pallas kernels for 0%

commit v1 on v0

--- a/solution.py
+++ b/solution.py
@@ -16,6 +16,35 @@
     return lax.ppermute(block, axis, route)
 
 
+def swap_pair(block):
+    return lax.ppermute(block, "tp", [(0, 1), (1, 0)])
+
+
+def join_pair(block, axis):
+    other = swap_pair(block)
+    first = lax.axis_index("tp") == 0
+    low = jnp.where(first, block, other)
+    high = jnp.where(first, other, block)
+    return jnp.concatenate([low, high], axis=axis)
+
+
+def scatter_sum(partial):
+    device_count = lax.axis_size("sp")
+    inner = 1
+    while inner * inner < device_count:
+        inner *= 2
+    outer = device_count // inner
+    near = [[o * inner + k for k in range(inner)] for o in range(outer)]
+    far = [[o * inner + k for o in range(outer)] for k in range(inner)]
+    rows = partial.shape[0] // device_count
+    cols = partial.shape[1]
+    blocks = partial.astype(jnp.bfloat16).reshape(outer, inner, rows, cols).transpose(1, 0, 2, 3)
+    moved = lax.all_to_all(blocks, "sp", 0, 0, tiled=True, axis_index_groups=near)
+    part = jnp.sum(moved.astype(jnp.float32), axis=0).astype(jnp.bfloat16)
+    moved = lax.all_to_all(part, "sp", 0, 0, tiled=True, axis_index_groups=far)
+    return jnp.sum(moved.astype(jnp.float32), axis=0)
+
+
 def silu_parts(pre):
     sigma = jax.nn.sigmoid(pre)
     return (pre * sigma, sigma * (1.0 + pre * (1.0 - sigma)))
@@ -34,25 +63,22 @@
 
 
 def expert_pass(token_rows, cot_rows, expert_gate, expert_up, expert_down):
-    moved_tokens, moved_cots = (
-        lax.all_to_all(token_rows, "sp", split_axis=0, concat_axis=0, tiled=True),
-        lax.all_to_all(cot_rows, "sp", split_axis=0, concat_axis=0, tiled=True),
-    )
-    full_tokens, full_cots = (
-        lax.all_gather(moved_tokens, "tp", axis=2, tiled=True),
-        lax.all_gather(moved_cots, "tp", axis=2, tiled=True),
-    )
+    moved_tokens = lax.all_to_all(token_rows, "sp", split_axis=0, concat_axis=0, tiled=True)
+    moved_cots = lax.all_to_all(cot_rows, "sp", split_axis=0, concat_axis=0, tiled=True)
+    full_tokens = join_pair(moved_tokens, 2)
     local_count = expert_gate.shape[0]
     source_count = full_tokens.shape[0] // local_count
     slot_count = full_tokens.shape[1]
     split_tokens = full_tokens.reshape(source_count, local_count, slot_count, D)
-    split_cots = full_cots.reshape(source_count, local_count, slot_count, D)
     tokens_in = split_tokens[:, 0].reshape(source_count * slot_count, D)
-    cots_in = split_cots[:, 0].reshape(source_count * slot_count, D)
     gate_w = expert_gate[0]
     up_w = expert_up[0]
     pre_gate = jnp.dot(tokens_in, gate_w, preferred_element_type=jnp.float32)
     pre_up = jnp.dot(tokens_in, up_w, preferred_element_type=jnp.float32)
+    pre_gate, pre_up, moved_cots = lax.optimization_barrier((pre_gate, pre_up, moved_cots))
+    full_cots = join_pair(moved_cots, 2)
+    split_cots = full_cots.reshape(source_count, local_count, slot_count, D)
+    cots_in = split_cots[:, 0].reshape(source_count * slot_count, D)
     active, slope = silu_parts(pre_gate)
     hidden = (active * pre_up).astype(jnp.bfloat16)
     down_grads = [contract_rows(hidden, cots_in)]
@@ -61,17 +87,25 @@
     d_up = (d_hidden * active).astype(jnp.bfloat16)
     gate_grads = [contract_rows(tokens_in, d_gate)]
     up_grads = [contract_rows(tokens_in, d_up)]
-    partial_term = contract_cols(d_gate, gate_w) + contract_cols(d_up, up_w)
-    partials = [partial_term.reshape(source_count, slot_count, D)]
-    stacked = jnp.stack(partials, axis=1).reshape(source_count * local_count, slot_count, D)
-    summed = lax.psum_scatter(stacked.astype(jnp.bfloat16), "tp", scatter_dimension=2, tiled=True)
+    half = D // 2
+    mine = lax.axis_index("tp") * half
+
+    def term(start):
+        gate_part = lax.dynamic_slice_in_dim(gate_w, start, half, axis=0)
+        up_part = lax.dynamic_slice_in_dim(up_w, start, half, axis=0)
+        product = contract_cols(d_gate, gate_part) + contract_cols(d_up, up_part)
+        return product.astype(jnp.bfloat16)
+
+    received = swap_pair(term(half - mine))
+    summed = (term(mine).astype(jnp.float32) + received.astype(jnp.float32)).astype(jnp.bfloat16)
+    summed = summed.reshape(source_count * local_count, slot_count, half)
     returned = lax.all_to_all(summed, "sp", split_axis=0, concat_axis=0, tiled=True)
     grads = (
         jnp.stack(gate_grads, axis=0),
         jnp.stack(up_grads, axis=0),
         jnp.stack(down_grads, axis=0),
     )
-    return (returned, grads)
+    return lax.optimization_barrier((returned, grads))
 
 
 def shards(
@@ -102,7 +136,6 @@
     inv_rms = lax.rsqrt(square_sum / D + epsilon)
     normed = (mid32 * inv_rms[:, None] * gain32).astype(jnp.bfloat16)
     shares = jnp.stack([group_prob * first_share, group_prob * (1.0 - first_share)], axis=1)
-    weighted = (layer_cot.astype(jnp.float32)[:, None, :] * shares[:, :, None]).astype(jnp.bfloat16)
     flat_ids = expert_ids.reshape(-1)
     pair_count = flat_ids.shape[0]
     onehot = (flat_ids[:, None] == jnp.arange(expert_count, dtype=jnp.int32)[None, :]).astype(
@@ -114,14 +147,17 @@
     source = jnp.full((expert_count * slot_count,), pair_count, jnp.int32)
     source = source.at[slot_index].set(jnp.arange(pair_count, dtype=jnp.int32))
     normed_pad = jnp.concatenate([normed, jnp.zeros((1, half_width), jnp.bfloat16)], axis=0)
-    weighted_pad = jnp.concatenate(
-        [weighted.reshape(pair_count, half_width), jnp.zeros((1, half_width), jnp.bfloat16)], axis=0
-    )
+    cot_pad = jnp.concatenate([layer_cot, jnp.zeros((1, half_width), jnp.bfloat16)], axis=0)
+    share_pad = jnp.concatenate([shares.reshape(-1), jnp.zeros((2,), jnp.float32)])
     token_rows = normed_pad[source // 2].reshape(expert_count, slot_count, half_width)
-    cot_rows = weighted_pad[source].reshape(expert_count, slot_count, half_width)
+    cot_rows = (cot_pad[source // 2].astype(jnp.float32) * share_pad[source][:, None]).astype(
+        jnp.bfloat16
+    )
+    cot_rows = cot_rows.reshape(expert_count, slot_count, half_width)
     back_rows, grads = expert_pass(token_rows, cot_rows, expert_gate, expert_up, expert_down)
-    picked = back_rows.reshape(expert_count * slot_count, half_width)[slot_index]
-    d_normed = jnp.sum(picked.astype(jnp.float32).reshape(row_count, 2, half_width), axis=1)
+    flat_back = back_rows.reshape(expert_count * slot_count, half_width)
+    slots = slot_index.reshape(row_count, 2)
+    d_normed = flat_back[slots[:, 0]].astype(jnp.float32) + flat_back[slots[:, 1]].astype(jnp.float32)
     g_dn = gain32 * d_normed
     inner = lax.psum(jnp.sum(mid32 * g_dn, axis=1), "tp") / D
     mid_total = (
@@ -130,7 +166,7 @@
         - mid32 * (inv_rms**3 * inner)[:, None]
     )
     mid_grad = mid_total.astype(jnp.bfloat16)
-    full_mid = lax.all_gather(mid_grad, "tp", axis=1, tiled=True)
+    full_mid = join_pair(mid_grad, 1)
     channel_count = b_gate.shape[1]
     b32 = b_gate.astype(jnp.float32)
     y32 = conv_out.astype(jnp.float32)
@@ -142,9 +178,7 @@
         .reshape(row_count, channel_count)
         .astype(jnp.bfloat16)
     )
-    grad_out_weight = lax.psum_scatter(
-        contract_rows(full_mid, conv_normed), "sp", scatter_dimension=0, tiled=True
-    )
+    grad_out_weight = scatter_sum(contract_rows(full_mid, conv_normed))
     d_normed_conv = jnp.dot(full_mid, out_weight, preferred_element_type=jnp.float32).reshape(
         grouped.shape
     )

time: 423 us -> 328 us (0.78)
  blocking collectives: 78 us -> 5.08 us
  waiting for transfers between devices: 206 us -> 148 us
  starting transfers between devices: 17.3 us -> 52.6 us
  other arithmetic: 18.8 us -> 32.3 us
  between operations: 14.3 us -> 1.24 us
    reduce_scatter x2 -> x0, waiting for transfers between devices: 79.9 us -> none  [the longest x1 65.7 us: shards(): lax.psum_scatter(contract_rows(full_mid, conv_normed), 'sp', scatter_dime...]
    all_to_all x1 -> x0, blocking collectives: 72.9 us -> none  [expert_pass(): lax.all_to_all(cot_rows, 'sp', split_axis=0, concat_axis=0, tiled=True)]
    all_to_all x0 -> x3, waiting for transfers between devices: none -> 67.9 us  [the longest x1 38.8 us: expert_pass(): lax.all_to_all(cot_rows, 'sp', split_axis=0, concat_axis=0, tiled=True)]
    all_to_all x0 -> x3, starting transfers between devices: none -> 28.6 us  [the longest x1 13 us: expert_pass(): lax.all_to_all(cot_rows, 'sp', split_axis=0, concat_axis=0, tiled=True)]
    all_to_all x1, waiting for transfers between devices: 51.8 us -> 31 us  [expert_pass(): lax.all_to_all(summed, 'sp', split_axis=0, concat_axis=0, tiled=True)]
    all_gather x3 -> x0, waiting for transfers between devices: 18.4 us -> none  [the longest x1 16.4 us: shards(): full_mid = lax.all_gather(mid_grad, 'tp', axis=1, tiled=True)]
    all_to_all x1, waiting for transfers between devices: 52 us -> 40.5 us  [expert_pass(): lax.all_to_all(token_rows, 'sp', split_axis=0, concat_axis=0, tiled=True)]
    ppermute x0 -> x4, waiting for transfers between devices: none -> 8.89 us  [swap_pair(): return lax.ppermute(block, 'tp', [(0, 1), (1, 0)])]
  transfers between devices with their start and end apart: 8 -> 10, of which waited for: 7 -> 8; matrix products, arithmetic and copies ran while one was open for 12% -> 19% of each run, Pallas kernels for 0% -> 0%
where the time goes in v1:
time: 328 us; the launch traced here: 327 us
  waiting for transfers between devices  148 us (45%)
  starting transfers between devices  52.6 us (16%)
  matrix products  51.5 us (16%)
  local copies, waits for them, and re-layouts  36.1 us (11%)
  other arithmetic  32.3 us (10%)
  blocking collectives  5.08 us (2%)
    all_to_all x1, waiting for transfers between devices, expert_pass(): lax.all_to_all(token_rows, 'sp', split_axis=0, concat_axis=0, tiled=True)  40.5 us
    all_to_all x1, waiting for transfers between devices, expert_pass(): lax.all_to_all(cot_rows, 'sp', split_axis=0, concat_axis=0, tiled=True)  38.8 us
    all_to_all x1, waiting for transfers between devices, expert_pass(): lax.all_to_all(summed, 'sp', split_axis=0, concat_axis=0, tiled=True)  31 us
    dot_general x4, matrix products, contract_rows(): lax.dot_general(left, right, (((0,), (0,)), ((), ())), preferred_element_...  22.3 us
    all_to_all x1, waiting for transfers between devices, scatter_sum(): lax.all_to_all(blocks, 'sp', 0, 0, tiled=True, axis_index_groups=near)  19.5 us
    dot_general x5, matrix products, contract_cols(): lax.dot_general(left, right, (((1,), (1,)), ((), ())), preferred_element_...  19.4 us
    all_to_all x1, starting transfers between devices, expert_pass(): lax.all_to_all(summed, 'sp', split_axis=0, concat_axis=0, tiled=True)  13.9 us
    all_to_all x1, starting transfers between devices, expert_pass(): lax.all_to_all(cot_rows, 'sp', split_axis=0, concat_axis=0, tiled=True)  13 us
  transfers between devices with their start and end apart: 10, of which 8 were waited for; matrix products, arithmetic and copies ran while one was open for 19% of the time, Pallas kernels for 0%

profile of v1, /device:TPU:0, one launch (start us, length us, event | category | flops | bytes accessed | tf_op | source)
XLA Modules:
  0.0 327.1 jit_solution(45332170682876417)
XLA Ops:
  1.9 1.4 reduce-window.6
  4.8 4.1 %scatter_custom_fusion = s32[1280]{0:T(1024)S(1)} fusion(s32[640]{0:T(1024)S(1)} %fusion.44, s32[640]{0:T(1024)S(1)} %iota.11, s32[]{:T(128)} %constant.57.clone.1), kind=kCustom, calls=%fused_computation.109 | custom fusion | bytes 5124 | tf_op jit(solution)/shard_map/scatter | solution.py:148
  8.9 1.3 fusion.8
  10.2 2.6 psum.14
  13.8 5.1 %gather_fusion = bf16[1280,1024]{1,0:T(8,128)(2,1)} fusion(bf16[321,1024]{1,0:T(8,128)(2,1)S(1)} %concatenate.21, s32[2048]{0:T(1024)S(1)} %get-tuple-element.50), kind=kCustom, calls=%fused_computation | custom fusion | bytes 5248000 | tf_op jit(solution)/shard_map/gather | solution.py:152
  18.9 8.4 %all-to-all-start = ((bf16[16,80,1024]{2,1,0:T(8,128)(2,1)}), bf16[16,80,1024]{2,1,0:T(8,128)(2,1)}, u32[]{:S(2)}, u32[]{:S(2)}) async-start(bf16[16,80,1024]{2,1,0:T(8,128)(2,1)} %bitcast.86), calls=%async_computation | async-start | bytes 5242880 | tf_op jit(solution)/shard_map/all_to_all | solution.py:66
  27.6 5.0 %gather_fusion.2 = f32[1280]{0:T(1024)S(1)} fusion(f32[642]{0:T(1024)S(1)} %concatenate.24, s32[2048]{0:T(1024)S(1)} %get-tuple-element.49), kind=kCustom, calls=%fused_computation.2 | custom fusion | bytes 15360 | tf_op jit(solution)/shard_map/gather | solution.py:153
  33.8 5.1 %gather_fusion.1 = bf16[1280,1024]{1,0:T(8,128)(2,1)} fusion(bf16[321,1024]{1,0:T(8,128)(2,1)S(1)} %concatenate.23, s32[2048]{0:T(1024)S(1)} %get-tuple-element.50), kind=kCustom, calls=%fused_computation.1 | custom fusion | bytes 5248000 | tf_op jit(solution)/shard_map/gather | solution.py:153
  38.9 40.5 %all-to-all-done = bf16[16,80,1024]{2,1,0:T(8,128)(2,1)} async-done(((bf16[16,80,1024]{2,1,0:T(8,128)(2,1)}), bf16[16,80,1024]{2,1,0:T(8,128)(2,1)}, u32[]{:S(2)}, u32[]{:S(2)}) %all-to-all-start) | async-done | bytes 2621472 | tf_op jit(solution)/shard_map/all_to_all | solution.py:66
  79.4 3.7 %fusion = bf16[16,80,1024]{2,1,0:T(8,128)(2,1)} fusion(bf16[16,80,1024]{2,1,0:T(8,128)(2,1)} %bitcast.87, f32[16,80]{1,0:T(8,128)S(1)} %mul.226), kind=kLoop, calls=%fused_computation.9 | loop fusion | flops 3932160 | bytes 5248000 | tf_op jit(solution)/shard_map/convert_element_type | solution.py:153
  83.1 13.0 %all-to-all-start.1 = ((bf16[16,80,1024]{2,1,0:T(8,128)(2,1)}), bf16[16,80,1024]{2,1,0:T(8,128)(2,1)}, u32[]{:S(2)}, u32[]{:S(2)}) async-start(bf16[16,80,1024]{2,1,0:T(8,128)(2,1)} %fusion), calls=%async_computation.1 | async-start | bytes 5242880 | tf_op jit(solution)/shard_map/all_to_all | solution.py:67
  96.2 2.9 broadcast_select_fusion.3
  100.6 4.5 %fusion.4 = f32[1280,512]{1,0:T(8,128)} fusion(bf16[1280,2048]{1,0:T(8,128)(2,1)S(1)} %bitcast.89, bf16[1,2048,512]{2,1,0:T(8,128)(2,1)S(1)} %copy-done.12), kind=kOutput, calls=%fused_computation.32 | convolution fusion | flops 2684354560 | bytes 9961472 | tf_op jit(solution)/shard_map/dot_general | solution.py:77
  105.1 4.4 %fusion.6 = f32[1280,512]{1,0:T(8,128)} fusion(bf16[1280,2048]{1,0:T(8,128)(2,1)S(1)} %bitcast.90, bf16[1,2048,512]{2,1,0:T(8,128)(2,1)S(1)} %copy-done), kind=kOutput, calls=%fused_computation.34 | convolution fusion | flops 2684354560 | bytes 9961472 | tf_op jit(solution)/shard_map/dot_general | solution.py:76
  109.5 38.8 %all-to-all-done.1 = bf16[16,80,1024]{2,1,0:T(8,128)(2,1)} async-done(((bf16[16,80,1024]{2,1,0:T(8,128)(2,1)}), bf16[16,80,1024]{2,1,0:T(8,128)(2,1)}, u32[]{:S(2)}, u32[]{:S(2)}) %all-to-all-start.1) | async-done | bytes 2621472 | tf_op jit(solution)/shard_map/all_to_all | solution.py:67
  148.3 5.2 %collective-permute-done.1 = bf16[16,80,1024]{2,1,0:T(8,128)(2,1)} collective-permute-done((bf16[16,80,1024]{2,1,0:T(8,128)(2,1)}, bf16[16,80,1024]{2,1,0:T(8,128)(2,1)}, u32[]{:S(2)}, u32[]{:S(2)}) %collective-permute-start.1) | collective-permute-done | bytes 2621472 | tf_op jit(solution)/shard_map/ppermute | solution.py:20
  153.6 2.9 broadcast_select_fusion.1
  158.1 6.8 %multiply_convert_fusion.1 = (bf16[1280,512]{1,0:T(8,128)(2,1)S(1)}, bf16[1280,512]{1,0:T(8,128)(2,1)S(1)}) fusion(f32[1280,512]{1,0:T(8,128)} %fusion.6, f32[1280,512]{1,0:T(8,128)} %fusion.4, bf16[1280,2048]{1,0:T(8,128)(2,1)S(1)} %bitcast.93, bf16[1,512,2048]{2,1,0:T(8,128)(2,1)S(1)} %copy-done.26), kind=kOutput, calls=%fused_computation.18 | convolution fusion | flops 2692874240 | bytes 15204352 | tf_op jit(solution)/shard_map/dot_general | solution.py:60
  164.9 1.6 fusion.15
  167.4 3.1 add_convert_fusion.1
  170.6 3.0 fusion.18
  173.7 2.0 collective-permute-done.2
  175.7 4.9 %add_convert_fusion = bf16[1280,1024]{1,0:T(8,128)(2,1)} fusion(bf16[1280,1024]{1,0:T(8,128)(2,1)} %collective-permute-done.2, f32[1280,1024]{1,0:T(8,128)S(1)} %fusion.18, bf16[1280,512]{1,0:T(8,128)(2,1)S(1)} %copy-done.4, bf16[1,2048,512]{2,1,0:T(8,128)(2,1)S(1)} %copy-done.14, s32[]{:T(128)S(6)} %select_n.80), kind=kOutput, calls=%fused_computation.10 | convolution fusion | flops 1350041600 | bytes 12845060 | tf_op jit(solution)/shard_map/dot_general | solution.py:60
  180.7 13.9 %all-to-all-start.2 = ((bf16[16,80,1024]{2,1,0:T(8,128)(2,1)}), bf16[16,80,1024]{2,1,0:T(8,128)(2,1)S(1)}, u32[]{:S(2)}, u32[]{:S(2)}) async-start(bf16[16,80,1024]{2,1,0:T(8,128)(2,1)} %bitcast.85), calls=%async_computation.2 | async-start | bytes 5242880 | tf_op jit(solution)/shard_map/all_to_all | solution.py:102
  194.5 1.2 fusion.33
  195.8 8.0 %convolution_bitcast_fusion.1 = f32[1,2048,512]{2,1,0:T(8,128)} fusion(bf16[1280,2048]{1,0:T(8,128)(2,1)} %bitcast.91, bf16[1280,512]{1,0:T(8,128)(2,1)} %copy-done.3), kind=kOutput, calls=%fused_computation.14 | convolution fusion | flops 2684354560 | bytes 10747904 | tf_op jit(solution)/shard_map/dot_general | solution.py:54
  203.8 7.2 %convolution_bitcast_fusion.2 = f32[1,2048,512]{2,1,0:T(8,128)} fusion(bf16[1280,2048]{1,0:T(8,128)(2,1)} %bitcast.92, bf16[1280,512]{1,0:T(8,128)(2,1)S(1)} %copy-done.29), kind=kOutput, calls=%fused_computation.15 | convolution fusion | flops 2684354560 | bytes 10747904 | tf_op jit(solution)/shard_map/dot_general | solution.py:54
  211.0 4.5 %convolution_bitcast_fusion = f32[1,512,2048]{2,1,0:T(8,128)} fusion(bf16[1280,2048]{1,0:T(8,128)(2,1)S(1)} %bitcast.96, f32[1280,512]{1,0:T(8,128)S(1)} %copy-done.30, f32[1280,512]{1,0:T(8,128)S(1)} %copy-done.31), kind=kOutput, calls=%fused_computation.13 | convolution fusion | flops 2688286720 | bytes 14680064 | tf_op jit(solution)/shard_map/dot_general | solution.py:54
  215.5 31.0 %all-to-all-done.2 = bf16[16,80,1024]{2,1,0:T(8,128)(2,1)S(1)} async-done(((bf16[16,80,1024]{2,1,0:T(8,128)(2,1)}), bf16[16,80,1024]{2,1,0:T(8,128)(2,1)S(1)}, u32[]{:S(2)}, u32[]{:S(2)}) %all-to-all-start.2) | async-done | bytes 2621472 | tf_op jit(solution)/shard_map/all_to_all | solution.py:102
  246.6 2.6 gather_fusion.3
  249.2 2.6 gather_fusion.4
  251.8 1.7 fusion.11
  253.6 2.5 psum.15
  256.1 2.0 fusion.13
  258.7 1.6 collective-permute-done.3
  260.3 1.2 broadcast_select_fusion.5
  264.5 2.7 convolution_convert_fusion
  267.1 1.6 copy.69
  268.7 6.8 %all-to-all-start.3 = ((bf16[4,4,128,512]{3,2,1,0:T(8,128)(2,1)}), bf16[4,4,128,512]{3,2,1,0:T(8,128)(2,1)S(1)}, u32[]{:S(2)}, u32[]{:S(2)}) async-start(bf16[4,4,128,512]{3,2,1,0:T(8,128)(2,1)} %bitcast.88), calls=%async_computation.3 | async-start | bytes 4194304 | tf_op jit(solution)/shard_map/all_to_all | solution.py:42
  277.3 2.6 convert_multiply_fusion.7
  279.9 1.4 collective-permute-start.4
  281.3 19.5 %all-to-all-done.3 = bf16[4,4,128,512]{3,2,1,0:T(8,128)(2,1)S(1)} async-done(((bf16[4,4,128,512]{3,2,1,0:T(8,128)(2,1)}), bf16[4,4,128,512]{3,2,1,0:T(8,128)(2,1)S(1)}, u32[]{:S(2)}, u32[]{:S(2)}) %all-to-all-start.3) | async-done | bytes 2097184 | tf_op jit(solution)/shard_map/all_to_all | solution.py:42
  300.8 1.3 reduce_sum.76
  302.0 8.7 %all-to-all-start.4 = ((bf16[4,128,512]{2,1,0:T(8,128)(2,1)}), bf16[4,128,512]{2,1,0:T(8,128)(2,1)}, u32[]{:S(2)}, u32[]{:S(2)}) async-start(bf16[4,128,512]{2,1,0:T(8,128)(2,1)} %reduce_sum.76), calls=%async_computation.4 | async-start | bytes 1048576 | tf_op jit(solution)/shard_map/all_to_all | solution.py:44
  310.7 2.0 fusion.29
  312.8 2.0 multiply_convert_fusion.4
  315.6 9.6 %all-to-all-done.4 = bf16[4,128,512]{2,1,0:T(8,128)(2,1)} async-done(((bf16[4,128,512]{2,1,0:T(8,128)(2,1)}), bf16[4,128,512]{2,1,0:T(8,128)(2,1)}, u32[]{:S(2)}, u32[]{:S(2)}) %all-to-all-start.4) | async-done | bytes 524320 | tf_op jit(solution)/shard_map/all_to_all | solution.py:44
  325.2 1.8 convert_reduce_fusion
  (121 shorter events, 15.6 us)
Async XLA Ops:
  0.6 104.5 %copy-start = (bf16[1,2048,512]{2,1,0:T(8,128)(2,1)S(1)}, bf16[1,2048,512]{2,1,0:T(8,128)(2,1)}, u32[]{:S(2)}) copy-start(bf16[1,2048,512]{2,1,0:T(8,128)(2,1)} %param.22) | copy-start | bytes 6291460
  0.6 12.9 %copy-start.2 = (bf16[320,1024]{1,0:T(8,128)(2,1)S(1)}, bf16[320,1024]{1,0:T(8,128)(2,1)}, u32[]{:S(2)}) copy-start(bf16[320,1024]{1,0:T(8,128)(2,1)} %param.16) | copy-start | bytes 1966084
  18.9 8.4 %copy-start.24 = (f32[320]{0:T(512)S(1)}, f32[320]{0:T(512)}, u32[]{:S(2)}) copy-start(f32[320]{0:T(512)} %param.20) | copy-start | bytes 3844
  18.9 8.4 %copy-start.25 = (f32[320]{0:T(512)S(1)}, f32[320]{0:T(512)}, u32[]{:S(2)}) copy-start(f32[320]{0:T(512)} %param.21) | copy-start | bytes 3844
  18.9 60.5 %all-to-all-start = ((bf16[16,80,1024]{2,1,0:T(8,128)(2,1)}), bf16[16,80,1024]{2,1,0:T(8,128)(2,1)}, u32[]{:S(2)}, u32[]{:S(2)}) async-start(bf16[16,80,1024]{2,1,0:T(8,128)(2,1)} %bitcast.86), calls=%async_computation | async-start | bytes 5242880 | tf_op jit(solution)/shard_map/all_to_all | solution.py:66
  79.4 16.8 %collective-permute-start = (bf16[16,80,1024]{2,1,0:T(8,128)(2,1)}, bf16[16,80,1024]{2,1,0:T(8,128)(2,1)}, u32[]{:S(2)}, u32[]{:S(2)}) collective-permute-start(bf16[16,80,1024]{2,1,0:T(8,128)(2,1)} %all-to-all-done), channel_id=1, source_target_pairs={{0,1},{1,0},{2,3},{3,2},{4,5},{5,4},{6,7},{7,6},{8,9},{9,8},{10,11... | collective-permute-start | bytes 7864328 | tf_op jit(solution)/shard_map/ppermute | solution.py:20
  83.1 65.2 %all-to-all-start.1 = ((bf16[16,80,1024]{2,1,0:T(8,128)(2,1)}), bf16[16,80,1024]{2,1,0:T(8,128)(2,1)}, u32[]{:S(2)}, u32[]{:S(2)}) async-start(bf16[16,80,1024]{2,1,0:T(8,128)(2,1)} %fusion), calls=%async_computation.1 | async-start | bytes 5242880 | tf_op jit(solution)/shard_map/all_to_all | solution.py:67
  99.0 1.6 copy-start.12
  99.7 5.4 %copy-start.5 = (bf16[16,80,2048]{2,1,0:T(8,128)(2,1)}, bf16[16,80,2048]{2,1,0:T(8,128)(2,1)S(1)}, u32[]{:S(2)}) copy-start(bf16[16,80,2048]{2,1,0:T(8,128)(2,1)S(1)} %pad_maximum_fusion) | copy-start | bytes 15728644
  148.3 5.3 %collective-permute-start.1 = (bf16[16,80,1024]{2,1,0:T(8,128)(2,1)}, bf16[16,80,1024]{2,1,0:T(8,128)(2,1)}, u32[]{:S(2)}, u32[]{:S(2)}) collective-permute-start(bf16[16,80,1024]{2,1,0:T(8,128)(2,1)} %all-to-all-done.1), channel_id=1, source_target_pairs={{0,1},{1,0},{2,3},{3,2},{4,5},{5,4},{6,7},{7,6},{8,9},{9,8},{10,11... | collective-permute-start | bytes 7864328 | tf_op jit(solution)/shard_map/ppermute | solution.py:20
  156.5 1.6 copy-start.26
  157.1 7.7 %copy-start.6 = (bf16[16,80,2048]{2,1,0:T(8,128)(2,1)}, bf16[16,80,2048]{2,1,0:T(8,128)(2,1)S(1)}, u32[]{:S(2)}) copy-start(bf16[16,80,2048]{2,1,0:T(8,128)(2,1)S(1)} %pad_maximum_fusion.1) | copy-start | bytes 15728644
  164.8 1.6 copy-start.28
  164.9 1.6 copy-start.3
  164.9 2.5 copy-start.13
  170.5 5.3 %collective-permute-start.2 = (bf16[1280,1024]{1,0:T(8,128)(2,1)}, bf16[1280,1024]{1,0:T(8,128)(2,1)}, u32[]{:S(2)}, u32[]{:S(2)}) collective-permute-start(bf16[1280,1024]{1,0:T(8,128)(2,1)} %add_convert_fusion.1), channel_id=1, source_target_pairs={{0,1},{1,0},{2,3},{3,2},{4,5},{5,4},{6,7},{7,6},{8,9},{9,8},{10,11... | collective-permute-start | bytes 7864328 | tf_op jit(solution)/shard_map/ppermute | solution.py:20
  170.6 5.1 %copy-start.4 = (bf16[1280,512]{1,0:T(8,128)(2,1)S(1)}, bf16[1280,512]{1,0:T(8,128)(2,1)}, u32[]{:S(2)}) copy-start(bf16[1280,512]{1,0:T(8,128)(2,1)} %copy-done.3) | copy-start | bytes 3932164
  170.6 5.1 %copy-start.14 = (bf16[1,2048,512]{2,1,0:T(8,128)(2,1)S(1)}, bf16[1,2048,512]{2,1,0:T(8,128)(2,1)}, u32[]{:S(2)}) copy-start(bf16[1,2048,512]{2,1,0:T(8,128)(2,1)} %param.23) | copy-start | bytes 6291460
  180.7 65.9 %all-to-all-start.2 = ((bf16[16,80,1024]{2,1,0:T(8,128)(2,1)}), bf16[16,80,1024]{2,1,0:T(8,128)(2,1)S(1)}, u32[]{:S(2)}, u32[]{:S(2)}) async-start(bf16[16,80,1024]{2,1,0:T(8,128)(2,1)} %bitcast.85), calls=%async_computation.2 | async-start | bytes 5242880 | tf_op jit(solution)/shard_map/all_to_all | solution.py:102
  195.8 8.0 %copy-start.29 = (bf16[1280,512]{1,0:T(8,128)(2,1)S(1)}, bf16[1280,512]{1,0:T(8,128)(2,1)}, u32[]{:S(2)}) copy-start(bf16[1280,512]{1,0:T(8,128)(2,1)} %copy-done.28) | copy-start | bytes 3932164
  195.8 15.2 %slice-start = ((s8[5242880]{0:T(1024)(128)(4,1)}), s8[4194304]{0:T(1024)(128)(4,1)S(1)}, s32[]{:S(2)}) async-start(s8[5242880]{0:T(1024)(128)(4,1)} %bitcast.94), calls=%async_computation.5 | async-start | bytes 8388608
  203.8 7.2 %slice-start.1 = ((s8[5242880]{0:T(1024)(128)(4,1)}), s8[1048576]{0:T(1024)(128)(4,1)S(1)}, s32[]{:S(2)}) async-start(s8[5242880]{0:T(1024)(128)(4,1)} %bitcast.94), calls=%async_computation.6 | async-start | bytes 2097152
  203.8 7.2 %copy-start.30 = (f32[1280,512]{1,0:T(8,128)S(1)}, f32[1280,512]{1,0:T(8,128)}, u32[]{:S(2)}) copy-start(f32[1280,512]{1,0:T(8,128)} %fusion.4) | copy-start | bytes 7864324
  203.8 7.2 %copy-start.31 = (f32[1280,512]{1,0:T(8,128)S(1)}, f32[1280,512]{1,0:T(8,128)}, u32[]{:S(2)}) copy-start(f32[1280,512]{1,0:T(8,128)} %fusion.6) | copy-start | bytes 7864324
  251.8 6.4 %copy-start.23 = (bf16[512]{0:T(512)(128)(2,1)S(1)}, bf16[512]{0:T(512)(128)(2,1)}, u32[]{:S(2)}) copy-start(bf16[512]{0:T(512)(128)(2,1)} %param.26) | copy-start | bytes 3076
  251.8 6.5 %copy-start.7 = (bf16[320,512]{1,0:T(8,128)(2,1)S(1)}, bf16[320,512]{1,0:T(8,128)(2,1)}, u32[]{:S(2)}) copy-start(bf16[320,512]{1,0:T(8,128)(2,1)} %param.30) | copy-start | bytes 983044
  251.8 6.5 %copy-start.15 = (bf16[320,512]{1,0:T(8,128)(2,1)S(1)}, bf16[320,512]{1,0:T(8,128)(2,1)}, u32[]{:S(2)}) copy-start(bf16[320,512]{1,0:T(8,128)(2,1)} %param.27) | copy-start | bytes 983044
  258.0 3.5 %copy-start.11 = (bf16[320,1024]{1,0:T(8,128)(2,1)}, bf16[320,1024]{1,0:T(8,128)(2,1)S(1)}, u32[]{:S(2)}) copy-start(bf16[320,1024]{1,0:T(8,128)(2,1)S(1)} %fusion.13) | copy-start | bytes 1966084
  258.0 2.3 collective-permute-start.3
  258.7 3.6 %copy-start.27 = (bf16[2048,512]{1,0:T(8,128)(2,1)S(1)}, bf16[2048,512]{1,0:T(8,128)(2,1)}, u32[]{:S(2)}) copy-start(bf16[2048,512]{1,0:T(8,128)(2,1)} %param.25) | copy-start | bytes 6291460
  261.5 0.9 copy-start.17
  263.2 0.9 copy-start.9
  263.3 1.2 copy-start.16
  264.5 2.7 copy-start.10
  268.7 6.8 %copy-start.19 = (bf16[3,512]{1,0:T(4,128)(2,1)S(1)}, bf16[3,512]{1,0:T(4,128)(2,1)}, u32[]{:S(2)}) copy-start(bf16[3,512]{1,0:T(4,128)(2,1)} %param.31) | copy-start | bytes 9220
  268.7 8.6 %copy-start.8 = (bf16[320,512]{1,0:T(8,128)(2,1)S(1)}, bf16[320,512]{1,0:T(8,128)(2,1)}, u32[]{:S(2)}) copy-start(bf16[320,512]{1,0:T(8,128)(2,1)} %param.30) | copy-start | bytes 983044
  268.7 32.1 %all-to-all-start.3 = ((bf16[4,4,128,512]{3,2,1,0:T(8,128)(2,1)}), bf16[4,4,128,512]{3,2,1,0:T(8,128)(2,1)S(1)}, u32[]{:S(2)}, u32[]{:S(2)}) async-start(bf16[4,4,128,512]{3,2,1,0:T(8,128)(2,1)} %bitcast.88), calls=%async_computation.3 | async-start | bytes 4194304 | tf_op jit(solution)/shard_map/all_to_all | solution.py:42
  279.9 32.9 %copy-start.20 = (f32[1,512]{1,0:T(1,128)S(1)}, f32[1,512]{1,0:T(1,128)}, u32[]{:S(2)}) copy-start(f32[1,512]{1,0:T(1,128)} %get-tuple-element.44) | copy-start | bytes 6148
  279.9 32.9 %copy-start.21 = (f32[1,512]{1,0:T(1,128)S(1)}, f32[1,512]{1,0:T(1,128)}, u32[]{:S(2)}) copy-start(f32[1,512]{1,0:T(1,128)} %get-tuple-element.45) | copy-start | bytes 6148
  279.9 32.9 %copy-start.22 = (f32[1,512]{1,0:T(1,128)S(1)}, f32[1,512]{1,0:T(1,128)}, u32[]{:S(2)}) copy-start(f32[1,512]{1,0:T(1,128)} %get-tuple-element.46) | copy-start | bytes 6148
  279.9 32.9 %collective-permute-start.4 = (f32[2,512]{1,0:T(2,128)S(1)}, f32[2,512]{1,0:T(2,128)S(1)}, u32[]{:S(2)}, u32[]{:S(2)}) collective-permute-start(f32[2,512]{1,0:T(2,128)S(1)} %slice.55), channel_id=1, source_target_pairs={{2,0},{4,2},{6,4},{8,6},{10,8},{12,10},{14,12},{16,14},{18,16},{20... | collective-permute-start | bytes 12296 | tf_op jit(solution)/shard_map/ppermute | solution.py:16
  302.0 12.8 %copy-start.18 = (bf16[320,512]{1,0:T(8,128)(2,1)S(1)}, bf16[320,512]{1,0:T(8,128)(2,1)}, u32[]{:S(2)}) copy-start(bf16[320,512]{1,0:T(8,128)(2,1)} %param.29) | copy-start | bytes 983044
  302.0 23.2 %all-to-all-start.4 = ((bf16[4,128,512]{2,1,0:T(8,128)(2,1)}), bf16[4,128,512]{2,1,0:T(8,128)(2,1)}, u32[]{:S(2)}, u32[]{:S(2)}) async-start(bf16[4,128,512]{2,1,0:T(8,128)(2,1)} %reduce_sum.76), calls=%async_computation.4 | async-start | bytes 1048576 | tf_op jit(solution)/shard_map/all_to_all | solution.py:44
  310.7 16.3 %copy-start.1 = (bf16[1,2048,512]{2,1,0:T(8,128)(2,1)S(1)}, bf16[1,2048,512]{2,1,0:T(8,128)(2,1)}, u32[]{:S(2)}) copy-start(bf16[1,2048,512]{2,1,0:T(8,128)(2,1)} %param.22) | copy-start | bytes 6291460

commit v2 on v1

--- a/solution.py
+++ b/solution.py
@@ -18,6 +18,18 @@
 
 def swap_pair(block):
     return lax.ppermute(block, "tp", [(0, 1), (1, 0)])
+
+
+def swap_half(block):
+    device_count = lax.axis_size("sp")
+    half = device_count // 2
+    return lax.ppermute(block, "sp", [(i, (i + half) % device_count) for i in range(device_count)])
+
+
+def within_half(rows):
+    half = lax.axis_size("sp") // 2
+    groups = [[h * half + i for i in range(half)] for h in range(2)]
+    return lax.all_to_all(rows, "sp", 0, 0, tiled=True, axis_index_groups=groups)
 
 
 def join_pair(block, axis):
@@ -63,8 +75,8 @@
 
 
 def expert_pass(token_rows, cot_rows, expert_gate, expert_up, expert_down):
-    moved_tokens = lax.all_to_all(token_rows, "sp", split_axis=0, concat_axis=0, tiled=True)
-    moved_cots = lax.all_to_all(cot_rows, "sp", split_axis=0, concat_axis=0, tiled=True)
+    moved_tokens = within_half(token_rows)
+    moved_cots = within_half(cot_rows)
     full_tokens = join_pair(moved_tokens, 2)
     local_count = expert_gate.shape[0]
     source_count = full_tokens.shape[0] // local_count
@@ -98,7 +110,8 @@
 
     received = swap_pair(term(half - mine))
     summed = (term(mine).astype(jnp.float32) + received.astype(jnp.float32)).astype(jnp.bfloat16)
-    summed = summed.reshape(source_count * local_count, slot_count, half)
+    summed = summed.reshape(source_count, 2, slot_count // 2, half).transpose(1, 0, 2, 3)
+    summed = summed.reshape(2 * source_count, slot_count // 2, half)
     returned = lax.all_to_all(summed, "sp", split_axis=0, concat_axis=0, tiled=True)
     grads = (
         jnp.stack(gate_grads, axis=0),
@@ -136,24 +149,33 @@
     inv_rms = lax.rsqrt(square_sum / D + epsilon)
     normed = (mid32 * inv_rms[:, None] * gain32).astype(jnp.bfloat16)
     shares = jnp.stack([group_prob * first_share, group_prob * (1.0 - first_share)], axis=1)
-    flat_ids = expert_ids.reshape(-1)
-    pair_count = flat_ids.shape[0]
-    onehot = (flat_ids[:, None] == jnp.arange(expert_count, dtype=jnp.int32)[None, :]).astype(
-        jnp.int32
-    )
-    before = jnp.cumsum(onehot, axis=0) - onehot
-    ranks = jnp.sum(before * onehot, axis=1)
-    slot_index = flat_ids * slot_count + ranks
-    source = jnp.full((expert_count * slot_count,), pair_count, jnp.int32)
-    source = source.at[slot_index].set(jnp.arange(pair_count, dtype=jnp.int32))
-    normed_pad = jnp.concatenate([normed, jnp.zeros((1, half_width), jnp.bfloat16)], axis=0)
-    cot_pad = jnp.concatenate([layer_cot, jnp.zeros((1, half_width), jnp.bfloat16)], axis=0)
-    share_pad = jnp.concatenate([shares.reshape(-1), jnp.zeros((2,), jnp.float32)])
-    token_rows = normed_pad[source // 2].reshape(expert_count, slot_count, half_width)
+    half_count = expert_count // 2
+    my_half = lax.axis_index("sp") // (lax.axis_size("sp") // 2)
+    both_ids = jnp.stack([expert_ids.reshape(-1), swap_half(expert_ids).reshape(-1)])
+    both_shares = jnp.concatenate([shares, swap_half(shares)]).reshape(-1)
+    pair_count = both_ids.shape[1]
+    onehot = (both_ids[:, :, None] == jnp.arange(expert_count, dtype=jnp.int32)).astype(jnp.int32)
+    before = jnp.cumsum(onehot, axis=1) - onehot
+    ranks = jnp.sum(before * onehot, axis=2)
+    slot_index = both_ids[0] * slot_count + ranks[0]
+    origin = jnp.stack([my_half, 1 - my_half])[:, None]
+    local_ids = both_ids - my_half * half_count
+    target = (local_ids * 2 + origin) * slot_count + ranks
+    row_total = expert_count * slot_count
+    inside = (local_ids >= 0) & (local_ids < half_count)
+    target = jnp.where(inside, target, row_total).reshape(-1)
+    source = jnp.full((row_total,), 2 * pair_count, jnp.int32)
+    source = source.at[target].set(jnp.arange(2 * pair_count, dtype=jnp.int32), mode="drop")
+    empty = jnp.zeros((1, half_width), jnp.bfloat16)
+    normed_pad = jnp.concatenate([normed, swap_half(normed), empty], axis=0)
+    normed_pad, late_cot = lax.optimization_barrier((normed_pad, layer_cot))
+    cot_pad = jnp.concatenate([layer_cot, swap_half(late_cot), empty], axis=0)
+    share_pad = jnp.concatenate([both_shares, jnp.zeros((2,), jnp.float32)])
+    token_rows = normed_pad[source // 2].reshape(half_count, 2 * slot_count, half_width)
     cot_rows = (cot_pad[source // 2].astype(jnp.float32) * share_pad[source][:, None]).astype(
         jnp.bfloat16
     )
-    cot_rows = cot_rows.reshape(expert_count, slot_count, half_width)
+    cot_rows = cot_rows.reshape(half_count, 2 * slot_count, half_width)
     back_rows, grads = expert_pass(token_rows, cot_rows, expert_gate, expert_up, expert_down)
     flat_back = back_rows.reshape(expert_count * slot_count, half_width)
     slots = slot_index.reshape(row_count, 2)

time: 328 us -> 330 us (level)
  starting transfers between devices: 52.6 us -> 47.3 us
  local copies, waits for them, and re-layouts: 36.1 us -> 40.3 us
  other arithmetic: 32.3 us -> 36.3 us
    all_to_all x2, waiting for transfers between devices: 79.3 us -> 18.8 us  [within_half(): lax.all_to_all(rows, 'sp', 0, 0, tiled=True, axis_index_groups=groups)]
    ppermute x0 -> x4, waiting for transfers between devices: none -> 60.4 us  [swap_half(): lax.ppermute(block, 'sp', [(i, (i + half) % device_count) for i in range(...]
    ppermute x0 -> x4, starting transfers between devices: none -> 7.4 us  [swap_half(): lax.ppermute(block, 'sp', [(i, (i + half) % device_count) for i in range(...]
    all_to_all x1, starting transfers between devices: 13.9 us -> 7.18 us  [expert_pass(): lax.all_to_all(summed, 'sp', split_axis=0, concat_axis=0, tiled=True)]
    all_to_all x2, starting transfers between devices: 21.4 us -> 15.4 us  [within_half(): lax.all_to_all(rows, 'sp', 0, 0, tiled=True, axis_index_groups=groups)]
  transfers between devices with their start and end apart: 10 -> 14, of which waited for: 8 -> 9; matrix products, arithmetic and copies ran while one was open for 19% -> 24% of each run, Pallas kernels for 0% -> 0%
where the time goes in v2:
time: 330 us; the launch traced here: 329 us
  waiting for transfers between devices  149 us (45%)
  matrix products  49.8 us (15%)
  starting transfers between devices  47.3 us (14%)
  local copies, waits for them, and re-layouts  40.3 us (12%)
  other arithmetic  36.3 us (11%)
  blocking collectives  4.93 us (1%)
    ppermute x4, waiting for transfers between devices, swap_half(): lax.ppermute(block, 'sp', [(i, (i + half) % device_count) for i in range(...  60.4 us
    all_to_all x1, waiting for transfers between devices, expert_pass(): lax.all_to_all(summed, 'sp', split_axis=0, concat_axis=0, tiled=True)  32 us
    dot_general x4, matrix products, contract_rows(): lax.dot_general(left, right, (((0,), (0,)), ((), ())), preferred_element_...  22.3 us
    all_to_all x1, waiting for transfers between devices, scatter_sum(): lax.all_to_all(blocks, 'sp', 0, 0, tiled=True, axis_index_groups=near)  19.5 us
    all_to_all x2, waiting for transfers between devices, within_half(): lax.all_to_all(rows, 'sp', 0, 0, tiled=True, axis_index_groups=groups)  18.8 us
    dot_general x5, matrix products, contract_cols(): lax.dot_general(left, right, (((1,), (1,)), ((), ())), preferred_element_...  17.7 us
    all_to_all x2, starting transfers between devices, within_half(): lax.all_to_all(rows, 'sp', 0, 0, tiled=True, axis_index_groups=groups)  15.4 us
    all_to_all x1, waiting for transfers between devices, scatter_sum(): moved = lax.all_to_all(part, 'sp', 0, 0, tiled=True, axis_index_groups=far)  9.66 us
  transfers between devices with their start and end apart: 14, of which 9 were waited for; matrix products, arithmetic and copies ran while one was open for 24% of the time, Pallas kernels for 0%

profile of v2, /device:TPU:0, one launch (start us, length us, event | category | flops | bytes accessed | tf_op | source)
XLA Modules:
  0.0 329.1 jit_solution(13468923317674512844)
XLA Ops:
  0.6 4.1 %collective-permute-start.1 = (s32[320,2]{0,1:T(2,128)}, s32[320,2]{0,1:T(2,128)S(1)}, u32[]{:S(2)}, u32[]{:S(2)}) collective-permute-start(s32[320,2]{0,1:T(2,128)} %param.19), channel_id=1, source_target_pairs={{0,16},{2,18},{4,20},{6,22},{8,24},{10,26},{12,28},{14,30},{16,0},... | collective-permute-start | bytes 7688 | tf_op jit(solution)/shard_map/ppermute | solution.py:26
  6.1 2.5 psum.14
  12.5 2.9 reduce-window.6
  15.8 5.2 %scatter_custom_fusion = s32[1280]{0:T(1024)S(1)} fusion(s32[1280]{0:T(1024)S(1)} %fusion.40, s32[1280]{0:T(1024)S(1)} %iota.8, s32[]{:T(128)} %constant.75.clone.1), kind=kCustom, calls=%fused_computation.115 | custom fusion | bytes 5124 | tf_op jit(solution)/shard_map/scatter | solution.py:168
  21.1 21.4 %collective-permute-done = bf16[320,1024]{1,0:T(8,128)(2,1)} collective-permute-done((bf16[320,1024]{1,0:T(8,128)(2,1)S(1)}, bf16[320,1024]{1,0:T(8,128)(2,1)}, u32[]{:S(2)}, u32[]{:S(2)}) %collective-permute-start) | collective-permute-done | bytes 655392 | tf_op jit(solution)/shard_map/ppermute | solution.py:26
  42.5 1.6 maximum_maximum_fusion
  44.1 5.1 %gather_fusion = bf16[1280,1024]{1,0:T(8,128)(2,1)} fusion(bf16[641,1024]{1,0:T(8,128)(2,1)S(1)} %maximum_maximum_fusion, s32[2048]{0:T(1024)S(1)} %pad_clamp_fusion.1), kind=kCustom, calls=%fused_computation | custom fusion | bytes 5248000 | tf_op jit(solution)/shard_map/gather | solution.py:174
  49.1 4.5 %all-to-all-start = ((bf16[8,160,1024]{2,1,0:T(8,128)(2,1)}), bf16[8,160,1024]{2,1,0:T(8,128)(2,1)}, u32[]{:S(2)}, u32[]{:S(2)}) async-start(bf16[8,160,1024]{2,1,0:T(8,128)(2,1)} %bitcast.100), calls=%async_computation | async-start | bytes 5242880 | tf_op jit(solution)/shard_map/all_to_all | solution.py:32
  54.6 2.2 collective-permute-start.4
  56.8 39.0 %collective-permute-done.4 = f32[320,2]{0,1:T(2,128)S(1)} collective-permute-done((f32[320,2]{0,1:T(2,128)S(1)}, f32[320,2]{0,1:T(2,128)S(1)}, u32[]{:S(2)}, u32[]{:S(2)}) %collective-permute-start.4) | collective-permute-done | bytes 2592 | tf_op jit(solution)/shard_map/ppermute | solution.py:26
  96.3 7.1 %gather_fusion.2 = f32[1280]{0:T(1024)S(1)} fusion(f32[1282]{0:T(1024)S(1)} %concatenate.29, s32[2048]{0:T(1024)S(1)} %pad_clamp_fusion), kind=kCustom, calls=%fused_computation.2 | custom fusion | bytes 15360 | tf_op jit(solution)/shard_map/gather | solution.py:175
  103.6 1.6 maximum_maximum_fusion.1
  105.1 5.1 %gather_fusion.1 = bf16[1280,1024]{1,0:T(8,128)(2,1)} fusion(bf16[641,1024]{1,0:T(8,128)(2,1)S(1)} %maximum_maximum_fusion.1, s32[2048]{0:T(1024)S(1)} %pad_clamp_fusion.1), kind=kCustom, calls=%fused_computation.1 | custom fusion | bytes 5248000 | tf_op jit(solution)/shard_map/gather | solution.py:175
  110.2 3.7 %fusion = bf16[8,160,1024]{2,1,0:T(8,128)(2,1)} fusion(bf16[8,160,1024]{2,1,0:T(8,128)(2,1)} %bitcast.101, f32[8,160]{1,0:T(8,128)S(1)} %mul.254), kind=kLoop, calls=%fused_computation.9 | loop fusion | flops 3932160 | bytes 5248000 | tf_op jit(solution)/shard_map/convert_element_type | solution.py:175
  113.9 10.9 %all-to-all-start.1 = ((bf16[8,160,1024]{2,1,0:T(8,128)(2,1)}), bf16[8,160,1024]{2,1,0:T(8,128)(2,1)}, u32[]{:S(2)}, u32[]{:S(2)}) async-start(bf16[8,160,1024]{2,1,0:T(8,128)(2,1)} %fusion), calls=%async_computation.1 | async-start | bytes 5242880 | tf_op jit(solution)/shard_map/all_to_all | solution.py:32
  124.8 2.9 broadcast_select_fusion.3
  129.3 4.5 %fusion.4 = f32[1280,512]{1,0:T(8,128)} fusion(bf16[1280,2048]{1,0:T(8,128)(2,1)S(1)} %bitcast.103, bf16[1,2048,512]{2,1,0:T(8,128)(2,1)S(1)} %copy-done.13), kind=kOutput, calls=%fused_computation.32 | convolution fusion | flops 2684354560 | bytes 9961472 | tf_op jit(solution)/shard_map/dot_general | solution.py:89
  133.8 4.4 %fusion.6 = f32[1280,512]{1,0:T(8,128)} fusion(bf16[1280,2048]{1,0:T(8,128)(2,1)S(1)} %bitcast.104, bf16[1,2048,512]{2,1,0:T(8,128)(2,1)S(1)} %copy-done), kind=kOutput, calls=%fused_computation.34 | convolution fusion | flops 2684354560 | bytes 9961472 | tf_op jit(solution)/shard_map/dot_general | solution.py:88
  138.2 18.8 %all-to-all-done.1 = bf16[8,160,1024]{2,1,0:T(8,128)(2,1)} async-done(((bf16[8,160,1024]{2,1,0:T(8,128)(2,1)}), bf16[8,160,1024]{2,1,0:T(8,128)(2,1)}, u32[]{:S(2)}, u32[]{:S(2)}) %all-to-all-start.1) | async-done | bytes 2621472 | tf_op jit(solution)/shard_map/all_to_all | solution.py:32
  157.0 5.2 %collective-permute-done.5 = bf16[8,160,1024]{2,1,0:T(8,128)(2,1)} collective-permute-done((bf16[8,160,1024]{2,1,0:T(8,128)(2,1)}, bf16[8,160,1024]{2,1,0:T(8,128)(2,1)}, u32[]{:S(2)}, u32[]{:S(2)}) %collective-permute-start.5) | collective-permute-done | bytes 2621472 | tf_op jit(solution)/shard_map/ppermute | solution.py:20
  162.2 2.9 broadcast_select_fusion.1
  166.7 6.5 %multiply_convert_fusion.1 = (bf16[1280,512]{1,0:T(8,128)(2,1)S(1)}, bf16[1280,512]{1,0:T(8,128)(2,1)S(1)}) fusion(f32[1280,512]{1,0:T(8,128)} %fusion.6, f32[1280,512]{1,0:T(8,128)} %fusion.4, bf16[1280,2048]{1,0:T(8,128)(2,1)S(1)} %bitcast.107, bf16[1,512,2048]{2,1,0:T(8,128)(2,1)S(1)} %copy-done.28), kind=kOutput, calls=%fused_computation.18 | convolution fusion | flops 2692874240 | bytes 15204352 | tf_op jit(solution)/shard_map/dot_general | solution.py:72
  173.3 1.6 fusion.15
  175.8 3.0 add_convert_fusion.1
  179.0 3.0 fusion.18
  182.1 2.1 collective-permute-done.6
  184.1 3.5 %add_convert_fusion = bf16[1280,1024]{1,0:T(8,128)(2,1)S(1)} fusion(bf16[1280,1024]{1,0:T(8,128)(2,1)} %collective-permute-done.6, f32[1280,1024]{1,0:T(8,128)S(1)} %fusion.18, bf16[1280,512]{1,0:T(8,128)(2,1)S(1)} %get-tuple-element.34, bf16[1,2048,512]{2,1,0:T(8,128)(2,1)S(1)} %copy-done.15, s32[]{:T(128)S(6)} %select_n.99), kind=kOutput, calls=%fused_computation.10 | convolution fusion | flops 1350041600 | bytes 12845060 | tf_op jit(solution)/shard_map/dot_general | solution.py:72
  187.6 1.8 copy.98
  189.4 7.2 %all-to-all-start.2 = ((bf16[16,80,1024]{2,1,0:T(8,128)(2,1)}), bf16[16,80,1024]{2,1,0:T(8,128)(2,1)S(1)}, u32[]{:S(2)}, u32[]{:S(2)}) async-start(bf16[16,80,1024]{2,1,0:T(8,128)(2,1)} %bitcast.98), calls=%async_computation.2 | async-start | bytes 5242880 | tf_op jit(solution)/shard_map/all_to_all | solution.py:115
  196.9 8.0 %convolution_bitcast_fusion.1 = f32[1,2048,512]{2,1,0:T(8,128)} fusion(bf16[1280,2048]{1,0:T(8,128)(2,1)} %bitcast.105, bf16[1280,512]{1,0:T(8,128)(2,1)} %copy-done.3), kind=kOutput, calls=%fused_computation.14 | convolution fusion | flops 2684354560 | bytes 10747904 | tf_op jit(solution)/shard_map/dot_general | solution.py:66
  204.9 7.2 %convolution_bitcast_fusion.2 = f32[1,2048,512]{2,1,0:T(8,128)} fusion(bf16[1280,2048]{1,0:T(8,128)(2,1)} %bitcast.106, bf16[1280,512]{1,0:T(8,128)(2,1)S(1)} %copy-done.31), kind=kOutput, calls=%fused_computation.15 | convolution fusion | flops 2684354560 | bytes 10747904 | tf_op jit(solution)/shard_map/dot_general | solution.py:66
  212.1 4.5 %convolution_bitcast_fusion = f32[1,512,2048]{2,1,0:T(8,128)} fusion(bf16[1280,2048]{1,0:T(8,128)(2,1)S(1)} %bitcast.110, f32[1280,512]{1,0:T(8,128)S(1)} %copy-done.32, f32[1280,512]{1,0:T(8,128)S(1)} %copy-done.33), kind=kOutput, calls=%fused_computation.13 | convolution fusion | flops 2688286720 | bytes 14680064 | tf_op jit(solution)/shard_map/dot_general | solution.py:66
  216.6 32.0 %all-to-all-done.2 = bf16[16,80,1024]{2,1,0:T(8,128)(2,1)S(1)} async-done(((bf16[16,80,1024]{2,1,0:T(8,128)(2,1)}), bf16[16,80,1024]{2,1,0:T(8,128)(2,1)S(1)}, u32[]{:S(2)}, u32[]{:S(2)}) %all-to-all-start.2) | async-done | bytes 2621472 | tf_op jit(solution)/shard_map/all_to_all | solution.py:115
  248.6 2.6 gather_fusion.3
  251.2 2.6 gather_fusion.4
  253.9 1.7 fusion.11
  255.6 2.5 psum.15
  258.1 2.0 fusion.13
  260.8 1.6 collective-permute-done.7
  266.5 2.7 convolution_convert_fusion
  270.8 6.8 %all-to-all-start.3 = ((bf16[4,4,128,512]{3,2,1,0:T(8,128)(2,1)}), bf16[4,4,128,512]{3,2,1,0:T(8,128)(2,1)S(1)}, u32[]{:S(2)}, u32[]{:S(2)}) async-start(bf16[4,4,128,512]{3,2,1,0:T(8,128)(2,1)} %bitcast.102), calls=%async_computation.3 | async-start | bytes 4194304 | tf_op jit(solution)/shard_map/all_to_all | solution.py:54
  279.3 2.6 convert_multiply_fusion.7
  283.4 19.5 %all-to-all-done.3 = bf16[4,4,128,512]{3,2,1,0:T(8,128)(2,1)S(1)} async-done(((bf16[4,4,128,512]{3,2,1,0:T(8,128)(2,1)}), bf16[4,4,128,512]{3,2,1,0:T(8,128)(2,1)S(1)}, u32[]{:S(2)}, u32[]{:S(2)}) %all-to-all-start.3) | async-done | bytes 2097184 | tf_op jit(solution)/shard_map/all_to_all | solution.py:54
  304.1 8.6 %all-to-all-start.4 = ((bf16[4,128,512]{2,1,0:T(8,128)(2,1)}), bf16[4,128,512]{2,1,0:T(8,128)(2,1)}, u32[]{:S(2)}, u32[]{:S(2)}) async-start(bf16[4,128,512]{2,1,0:T(8,128)(2,1)} %reduce_sum.73), calls=%async_computation.4 | async-start | bytes 1048576 | tf_op jit(solution)/shard_map/all_to_all | solution.py:56
  312.7 2.0 fusion.29
  314.8 2.0 multiply_convert_fusion.4
  317.6 9.7 %all-to-all-done.4 = bf16[4,128,512]{2,1,0:T(8,128)(2,1)} async-done(((bf16[4,128,512]{2,1,0:T(8,128)(2,1)}), bf16[4,128,512]{2,1,0:T(8,128)(2,1)}, u32[]{:S(2)}, u32[]{:S(2)}) %all-to-all-start.4) | async-done | bytes 524320 | tf_op jit(solution)/shard_map/all_to_all | solution.py:56
  327.2 1.8 convert_reduce_fusion
  (149 shorter events, 23.2 us)
Async XLA Ops:
  0.6 133.2 %copy-start = (bf16[1,2048,512]{2,1,0:T(8,128)(2,1)S(1)}, bf16[1,2048,512]{2,1,0:T(8,128)(2,1)}, u32[]{:S(2)}) copy-start(bf16[1,2048,512]{2,1,0:T(8,128)(2,1)} %param.22) | copy-start | bytes 6291460
  0.6 11.3 %collective-permute-start.1 = (s32[320,2]{0,1:T(2,128)}, s32[320,2]{0,1:T(2,128)S(1)}, u32[]{:S(2)}, u32[]{:S(2)}) collective-permute-start(s32[320,2]{0,1:T(2,128)} %param.19), channel_id=1, source_target_pairs={{0,16},{2,18},{4,20},{6,22},{8,24},{10,26},{12,28},{14,30},{16,0},... | collective-permute-start | bytes 7688 | tf_op jit(solution)/shard_map/ppermute | solution.py:26
  10.6 10.6 %copy-start.10 = (bf16[320,1024]{1,0:T(8,128)(2,1)}, bf16[320,1024]{1,0:T(8,128)(2,1)S(1)}, u32[]{:S(2)}) copy-start(bf16[320,1024]{1,0:T(8,128)(2,1)S(1)} %fusion.10) | copy-start | bytes 1966084
  10.6 31.9 %collective-permute-start = (bf16[320,1024]{1,0:T(8,128)(2,1)S(1)}, bf16[320,1024]{1,0:T(8,128)(2,1)}, u32[]{:S(2)}, u32[]{:S(2)}) collective-permute-start(bf16[320,1024]{1,0:T(8,128)(2,1)S(1)} %fusion.10), channel_id=1, source_target_pairs={{0,16},{2,18},{4,20},{6,22},{8,24},{10,26},{12,28},{14,30},{16,0},... | collective-permute-start | bytes 1966088 | tf_op jit(solution)/shard_map/ppermute | solution.py:26
  49.1 4.5 %copy-start.11 = (bf16[320,1024]{1,0:T(8,128)(2,1)S(1)}, bf16[320,1024]{1,0:T(8,128)(2,1)}, u32[]{:S(2)}) copy-start(bf16[320,1024]{1,0:T(8,128)(2,1)} %param.17) | copy-start | bytes 1966084
  49.1 5.4 %copy-start.26 = (f32[320]{0:T(512)S(1)}, f32[320]{0:T(512)}, u32[]{:S(2)}) copy-start(f32[320]{0:T(512)} %param.20) | copy-start | bytes 3844
  49.1 5.4 %copy-start.27 = (f32[320]{0:T(512)S(1)}, f32[320]{0:T(512)}, u32[]{:S(2)}) copy-start(f32[320]{0:T(512)} %param.21) | copy-start | bytes 3844
  49.1 54.4 %all-to-all-start = ((bf16[8,160,1024]{2,1,0:T(8,128)(2,1)}), bf16[8,160,1024]{2,1,0:T(8,128)(2,1)}, u32[]{:S(2)}, u32[]{:S(2)}) async-start(bf16[8,160,1024]{2,1,0:T(8,128)(2,1)} %bitcast.100), calls=%async_computation | async-start | bytes 5242880 | tf_op jit(solution)/shard_map/all_to_all | solution.py:32
  53.7 49.9 %collective-permute-start.3 = (bf16[320,1024]{1,0:T(8,128)(2,1)S(1)}, bf16[320,1024]{1,0:T(8,128)(2,1)}, u32[]{:S(2)}, u32[]{:S(2)}) collective-permute-start(bf16[320,1024]{1,0:T(8,128)(2,1)S(1)} %copy-done.11), channel_id=1, source_target_pairs={{0,16},{2,18},{4,20},{6,22},{8,24},{10,26},{12,28},{14,30},{16,0},... | collective-permute-start | bytes 1966088 | tf_op jit(solution)/shard_map/ppermute | solution.py:26
  54.6 41.3 %collective-permute-start.4 = (f32[320,2]{0,1:T(2,128)S(1)}, f32[320,2]{0,1:T(2,128)S(1)}, u32[]{:S(2)}, u32[]{:S(2)}) collective-permute-start(f32[320,2]{0,1:T(2,128)S(1)} %pad_maximum_fusion.7), channel_id=1, source_target_pairs={{0,16},{2,18},{4,20},{6,22},{8,24},{10,26},{12,28},{14,30},{16,0},... | collective-permute-start | bytes 7688 | tf_op jit(solution)/shard_map/ppermute | solution.py:26
  103.5 21.3 %collective-permute-start.2 = (bf16[8,160,1024]{2,1,0:T(8,128)(2,1)}, bf16[8,160,1024]{2,1,0:T(8,128)(2,1)}, u32[]{:S(2)}, u32[]{:S(2)}) collective-permute-start(bf16[8,160,1024]{2,1,0:T(8,128)(2,1)} %all-to-all-done), channel_id=1, source_target_pairs={{0,1},{1,0},{2,3},{3,2},{4,5},{5,4},{6,7},{7,6},{8,9},{9,8},{10,11... | collective-permute-start | bytes 7864328 | tf_op jit(solution)/shard_map/ppermute | solution.py:20
  113.9 43.1 %all-to-all-start.1 = ((bf16[8,160,1024]{2,1,0:T(8,128)(2,1)}), bf16[8,160,1024]{2,1,0:T(8,128)(2,1)}, u32[]{:S(2)}, u32[]{:S(2)}) async-start(bf16[8,160,1024]{2,1,0:T(8,128)(2,1)} %fusion), calls=%async_computation.1 | async-start | bytes 5242880 | tf_op jit(solution)/shard_map/all_to_all | solution.py:32
  127.7 1.6 copy-start.13
  128.3 5.5 %copy-start.4 = (bf16[8,160,2048]{2,1,0:T(8,128)(2,1)}, bf16[8,160,2048]{2,1,0:T(8,128)(2,1)S(1)}, u32[]{:S(2)}) copy-start(bf16[8,160,2048]{2,1,0:T(8,128)(2,1)S(1)} %pad_maximum_fusion) | copy-start | bytes 15728644
  157.0 5.3 %collective-permute-start.5 = (bf16[8,160,1024]{2,1,0:T(8,128)(2,1)}, bf16[8,160,1024]{2,1,0:T(8,128)(2,1)}, u32[]{:S(2)}, u32[]{:S(2)}) collective-permute-start(bf16[8,160,1024]{2,1,0:T(8,128)(2,1)} %all-to-all-done.1), channel_id=1, source_target_pairs={{0,1},{1,0},{2,3},{3,2},{4,5},{5,4},{6,7},{7,6},{8,9},{9,8},{10,11... | collective-permute-start | bytes 7864328 | tf_op jit(solution)/shard_map/ppermute | solution.py:20
  165.1 1.6 copy-start.28
  165.8 7.5 %copy-start.5 = (bf16[8,160,2048]{2,1,0:T(8,128)(2,1)}, bf16[8,160,2048]{2,1,0:T(8,128)(2,1)S(1)}, u32[]{:S(2)}) copy-start(bf16[8,160,2048]{2,1,0:T(8,128)(2,1)S(1)} %pad_maximum_fusion.1) | copy-start | bytes 15728644
  173.3 1.6 copy-start.30
  173.3 10.9 %copy-start.3 = (bf16[1280,512]{1,0:T(8,128)(2,1)}, bf16[1280,512]{1,0:T(8,128)(2,1)S(1)}, u32[]{:S(2)}) copy-start(bf16[1280,512]{1,0:T(8,128)(2,1)S(1)} %get-tuple-element.34) | copy-start | bytes 3932164
  173.3 2.5 copy-start.14
  178.9 5.3 %collective-permute-start.6 = (bf16[1280,1024]{1,0:T(8,128)(2,1)}, bf16[1280,1024]{1,0:T(8,128)(2,1)}, u32[]{:S(2)}, u32[]{:S(2)}) collective-permute-start(bf16[1280,1024]{1,0:T(8,128)(2,1)} %add_convert_fusion.1), channel_id=1, source_target_pairs={{0,1},{1,0},{2,3},{3,2},{4,5},{5,4},{6,7},{7,6},{8,9},{9,8},{10,11... | collective-permute-start | bytes 7864328 | tf_op jit(solution)/shard_map/ppermute | solution.py:20
  179.0 5.1 %copy-start.15 = (bf16[1,2048,512]{2,1,0:T(8,128)(2,1)S(1)}, bf16[1,2048,512]{2,1,0:T(8,128)(2,1)}, u32[]{:S(2)}) copy-start(bf16[1,2048,512]{2,1,0:T(8,128)(2,1)} %param.23) | copy-start | bytes 6291460
  189.4 7.5 %copy-start.20 = (s32[320,2]{0,1:T(2,128)S(1)}, s32[320,2]{0,1:T(2,128)}, u32[]{:S(2)}) copy-start(s32[320,2]{0,1:T(2,128)} %param.19) | copy-start | bytes 7684
  189.4 59.2 %all-to-all-start.2 = ((bf16[16,80,1024]{2,1,0:T(8,128)(2,1)}), bf16[16,80,1024]{2,1,0:T(8,128)(2,1)S(1)}, u32[]{:S(2)}, u32[]{:S(2)}) async-start(bf16[16,80,1024]{2,1,0:T(8,128)(2,1)} %bitcast.98), calls=%async_computation.2 | async-start | bytes 5242880 | tf_op jit(solution)/shard_map/all_to_all | solution.py:115
  196.9 8.0 %copy-start.31 = (bf16[1280,512]{1,0:T(8,128)(2,1)S(1)}, bf16[1280,512]{1,0:T(8,128)(2,1)}, u32[]{:S(2)}) copy-start(bf16[1280,512]{1,0:T(8,128)(2,1)} %copy-done.30) | copy-start | bytes 3932164
  196.9 15.2 %slice-start = ((s8[5242880]{0:T(1024)(128)(4,1)}), s8[4194304]{0:T(1024)(128)(4,1)S(1)}, s32[]{:S(2)}) async-start(s8[5242880]{0:T(1024)(128)(4,1)} %bitcast.108), calls=%async_computation.5 | async-start | bytes 8388608
  204.9 7.2 %slice-start.1 = ((s8[5242880]{0:T(1024)(128)(4,1)}), s8[1048576]{0:T(1024)(128)(4,1)S(1)}, s32[]{:S(2)}) async-start(s8[5242880]{0:T(1024)(128)(4,1)} %bitcast.108), calls=%async_computation.6 | async-start | bytes 2097152
  204.9 7.2 %copy-start.32 = (f32[1280,512]{1,0:T(8,128)S(1)}, f32[1280,512]{1,0:T(8,128)}, u32[]{:S(2)}) copy-start(f32[1280,512]{1,0:T(8,128)} %fusion.4) | copy-start | bytes 7864324
  204.9 7.2 %copy-start.33 = (f32[1280,512]{1,0:T(8,128)S(1)}, f32[1280,512]{1,0:T(8,128)}, u32[]{:S(2)}) copy-start(f32[1280,512]{1,0:T(8,128)} %fusion.6) | copy-start | bytes 7864324
  251.2 2.6 copy-start.2
  253.9 6.5 %copy-start.25 = (bf16[512]{0:T(512)(128)(2,1)S(1)}, bf16[512]{0:T(512)(128)(2,1)}, u32[]{:S(2)}) copy-start(bf16[512]{0:T(512)(128)(2,1)} %param.26) | copy-start | bytes 3076
  253.9 6.5 %copy-start.6 = (bf16[320,512]{1,0:T(8,128)(2,1)S(1)}, bf16[320,512]{1,0:T(8,128)(2,1)}, u32[]{:S(2)}) copy-start(bf16[320,512]{1,0:T(8,128)(2,1)} %param.30) | copy-start | bytes 983044
  253.9 6.5 %copy-start.16 = (bf16[320,512]{1,0:T(8,128)(2,1)S(1)}, bf16[320,512]{1,0:T(8,128)(2,1)}, u32[]{:S(2)}) copy-start(bf16[320,512]{1,0:T(8,128)(2,1)} %param.27) | copy-start | bytes 983044
  260.1 3.5 %copy-start.12 = (bf16[320,1024]{1,0:T(8,128)(2,1)}, bf16[320,1024]{1,0:T(8,128)(2,1)S(1)}, u32[]{:S(2)}) copy-start(bf16[320,1024]{1,0:T(8,128)(2,1)S(1)} %fusion.13) | copy-start | bytes 1966084
  260.1 2.3 collective-permute-start.7
  260.8 3.7 %copy-start.29 = (bf16[2048,512]{1,0:T(8,128)(2,1)S(1)}, bf16[2048,512]{1,0:T(8,128)(2,1)}, u32[]{:S(2)}) copy-start(bf16[2048,512]{1,0:T(8,128)(2,1)} %param.25) | copy-start | bytes 6291460
  265.3 1.2 copy-start.17
  266.5 2.7 copy-start.9
  270.8 6.8 %copy-start.21 = (bf16[3,512]{1,0:T(4,128)(2,1)S(1)}, bf16[3,512]{1,0:T(4,128)(2,1)}, u32[]{:S(2)}) copy-start(bf16[3,512]{1,0:T(4,128)(2,1)} %param.31) | copy-start | bytes 9220
  270.8 8.6 %copy-start.7 = (bf16[320,512]{1,0:T(8,128)(2,1)S(1)}, bf16[320,512]{1,0:T(8,128)(2,1)}, u32[]{:S(2)}) copy-start(bf16[320,512]{1,0:T(8,128)(2,1)} %param.30) | copy-start | bytes 983044
  270.8 32.1 %all-to-all-start.3 = ((bf16[4,4,128,512]{3,2,1,0:T(8,128)(2,1)}), bf16[4,4,128,512]{3,2,1,0:T(8,128)(2,1)S(1)}, u32[]{:S(2)}, u32[]{:S(2)}) async-start(bf16[4,4,128,512]{3,2,1,0:T(8,128)(2,1)} %bitcast.102), calls=%async_computation.3 | async-start | bytes 4194304 | tf_op jit(solution)/shard_map/all_to_all | solution.py:54
  281.9 32.8 %copy-start.22 = (f32[1,512]{1,0:T(1,128)S(1)}, f32[1,512]{1,0:T(1,128)}, u32[]{:S(2)}) copy-start(f32[1,512]{1,0:T(1,128)} %get-tuple-element.46) | copy-start | bytes 6148
  281.9 32.8 %copy-start.23 = (f32[1,512]{1,0:T(1,128)S(1)}, f32[1,512]{1,0:T(1,128)}, u32[]{:S(2)}) copy-start(f32[1,512]{1,0:T(1,128)} %get-tuple-element.47) | copy-start | bytes 6148
  281.9 32.8 %copy-start.24 = (f32[1,512]{1,0:T(1,128)S(1)}, f32[1,512]{1,0:T(1,128)}, u32[]{:S(2)}) copy-start(f32[1,512]{1,0:T(1,128)} %get-tuple-element.48) | copy-start | bytes 6148
  281.9 32.8 %collective-permute-start.8 = (f32[2,512]{1,0:T(2,128)S(1)}, f32[2,512]{1,0:T(2,128)S(1)}, u32[]{:S(2)}, u32[]{:S(2)}) collective-permute-start(f32[2,512]{1,0:T(2,128)S(1)} %slice.61), channel_id=1, source_target_pairs={{2,0},{4,2},{6,4},{8,6},{10,8},{12,10},{14,12},{16,14},{18,16},{20... | collective-permute-start | bytes 12296 | tf_op jit(solution)/shard_map/ppermute | solution.py:16
  304.1 12.7 %copy-start.19 = (bf16[320,512]{1,0:T(8,128)(2,1)S(1)}, bf16[320,512]{1,0:T(8,128)(2,1)}, u32[]{:S(2)}) copy-start(bf16[320,512]{1,0:T(8,128)(2,1)} %param.29) | copy-start | bytes 983044
  304.1 23.2 %all-to-all-start.4 = ((bf16[4,128,512]{2,1,0:T(8,128)(2,1)}), bf16[4,128,512]{2,1,0:T(8,128)(2,1)}, u32[]{:S(2)}, u32[]{:S(2)}) async-start(bf16[4,128,512]{2,1,0:T(8,128)(2,1)} %reduce_sum.73), calls=%async_computation.4 | async-start | bytes 1048576 | tf_op jit(solution)/shard_map/all_to_all | solution.py:56
  312.7 16.4 %copy-start.1 = (bf16[1,2048,512]{2,1,0:T(8,128)(2,1)S(1)}, bf16[1,2048,512]{2,1,0:T(8,128)(2,1)}, u32[]{:S(2)}) copy-start(bf16[1,2048,512]{2,1,0:T(8,128)(2,1)} %param.22) | copy-start | bytes 6291460
  (2 other events, 1.7 us)
